TPU v7x, 32 devices: a whole 2x2x4 slice. The times are simulated.
32 devices in a mesh: sp: 8 (over z, y), tp: 4 (over x, core).
Axes of the slice: x: 2, y: 2, z: 4, core: 2. Of those that a mesh axis runs over, the one named last changes fastest.
Arguments:
- values_in: bfloat16 [4, 8192, 1024], P(None, 'sp', 'tp'), may hold values from -6 to 6
- gates_in: bfloat16 [4, 8192, 1024], P(None, 'sp', 'tp'), may hold values from -8 to 8
- conv_taps: bfloat16 [31, 1024], P(None, 'tp'), may hold values from -3 to 3
- conv_bias: bfloat16 [1024], P('tp'), may hold values from -3 to 3
- norm_gain: bfloat16 [1024], P('tp'), may hold values from 0.099609375 to 1.8984375
- out_weight: bfloat16 [1024, 4096], P('tp'), may hold values from -0.1875 to 0.1875
- out_grad: bfloat16 [4, 8192, 4096], P(None, 'sp'), may hold values from -1.5 to 1.5
Outputs:
- values_grad: bfloat16 [4, 8192, 1024], P(None, 'sp', 'tp')
- gates_grad: bfloat16 [4, 8192, 1024], P(None, 'sp', 'tp')
- taps_grad: float32 [31, 1024], P(None, 'tp')
- gain_grad: float32 [1024], P('tp')
- bias_grad: float32 [1024], P('tp')
- weight_grad: float32 [1024, 4096], P(('tp', 'sp'))
All inputs are finite; a program needn't handle non-finite values.
Results may differ from a plain program's by a relative error of at most 0.0048.
Values may be sent and summed in bfloat16 or wider, within the bound.
A program may use at most 128 MiB of HBM per device.

v0:
```python
import functools

import jax
import jax.numpy as jnp
from jax import lax
from jax.experimental import pallas as pl
from jax.experimental.pallas import tpu as pltpu
from jax.sharding import PartitionSpec as P

K = 31
EPS = 1e-05
HALO = 32
PAIR = 2
LANES = 128
F32 = jnp.float32
BF16 = jnp.bfloat16
VMEM_LIMIT = 60 * 1024 * 1024


def sigmoid(x):
    return 0.5 * jnp.tanh(0.5 * x) + 0.5


def peer_id(axis, distance):
    devices = lax.axis_size(axis)
    return {axis: lax.rem(lax.axis_index(axis) + distance, devices)}


def greet(pairs):
    barrier = pltpu.get_barrier_semaphore()
    for axis, distance in pairs:
        pl.semaphore_signal(
            barrier, inc=1, device_id=peer_id(axis, distance),
            device_id_type=pl.DeviceIdType.MESH,
        )
    pl.semaphore_wait(barrier, len(pairs))


def remote(src, dst, send_sem, recv_sem, axis, distance):
    return pltpu.make_async_remote_copy(
        src_ref=src, dst_ref=dst, send_sem=send_sem, recv_sem=recv_sem,
        device_id=peer_id(axis, distance), device_id_type=pl.DeviceIdType.MESH,
    )


def fir(x_ref, w_ref, lane_block, start, taps, blocks, init):
    accs = [init] * blocks
    x_block, w_block = lane_block
    weights = [w_ref[w_block, k] for k in taps]
    for offset in range(K + 8 * (blocks - 1)):
        piece = x_ref[x_block, pl.ds(start + offset, 8), :]
        for a in range(blocks):
            k = offset - 8 * a
            if 0 <= k < K:
                term = weights[k] * piece
                accs[a] = term if accs[a] is None else accs[a] + term
    return accs


def lane_sums(x):
    return jnp.sum(x.T, axis=0, keepdims=True)


def row_spread(row):
    return jnp.broadcast_to(row, (LANES, LANES)).T


def forward_kernel(
    seqs, seq_blocks, values_ref, gates_ref, values_before_ref, gates_before_ref, values_hbm,
    gates_hbm, raw_taps_ref, bias_ref, cot_ref, weight_ref,
    conv_ref, grad_ref, sums_ref, halo_ref, taps_ref, padded, values_halo, gates_halo, send_sems, recv_sems,
):
    step = pl.program_id(0)
    rows, chans = values_ref.shape
    lane_blocks = chans // LANES
    chunks = rows // LANES
    depth = cot_ref.shape[1] // chunks
    seq = lax.rem(step, seqs)
    part = seq_blocks - 1 - step // seqs
    block = seq * seq_blocks + part
    sp_devices = lax.axis_size("sp")
    tail = pl.ds(values_hbm.shape[1] - HALO, HALO)
    copies = [
        remote(src.at[:, tail], dst, send_sems.at[n], recv_sems.at[n], "sp", 1)
        for n, (src, dst) in enumerate(((values_hbm, values_halo), (gates_hbm, gates_halo)))
    ]

    @pl.when(step == 0)
    def _():
        greet((("sp", 1), ("sp", sp_devices - 1)))
        for copy in copies:
            copy.start()
        rows_of_taps = raw_taps_ref[...].astype(F32)
        for h in range(lane_blocks):
            for k in range(K):
                taps_ref[h, k] = jnp.broadcast_to(
                    rows_of_taps[k : k + 1, h * LANES : (h + 1) * LANES], (8, LANES)
                )

    @pl.when(step == seqs * (seq_blocks - 1))
    def _():
        for copy in copies:
            copy.wait()

    grad_ref[...] = jnp.zeros_like(grad_ref)

    def fill(values, gates, keep):
        for h in range(lane_blocks):
            lanes = slice(h * LANES, (h + 1) * LANES)
            sig = sigmoid(gates[:, lanes].astype(F32))
            gated = (values[:, lanes].astype(F32) * sig).astype(BF16).astype(F32)
            padded[h, :HALO, :] = gated * keep

    @pl.when(part == 0)
    def _():
        keep = jnp.where(lax.axis_index("sp") > 0, 1.0, 0.0).astype(F32)
        fill(values_halo[seq], gates_halo[seq], keep)
        for h in range(lane_blocks):
            halo_ref[seq, :, h * LANES : (h + 1) * LANES] = padded[h, :HALO, :]

    @pl.when(part != 0)
    def _():
        fill(values_before_ref[...], gates_before_ref[...], 1.0)

    def chunk(i, carry):
        first = pl.multiple_of(i * LANES, LANES)
        here = pl.ds(first, LANES)
        columns = pl.ds(pl.multiple_of(i * depth, depth), depth)
        grad_ref[...] += lax.dot_general(
            cot_ref[:, columns], weight_ref[:, columns], (((1,), (1,)), ((), ())),
            preferred_element_type=F32,
        )
        total = None
        for h in range(lane_blocks):
            lanes = slice(h * LANES, (h + 1) * LANES)
            sig = sigmoid(gates_ref[here, lanes].astype(F32))
            gated = (values_ref[here, lanes].astype(F32) * sig).astype(BF16).astype(F32)
            padded[h, pl.ds(first + HALO, LANES), :] = gated
            bias = jnp.broadcast_to(bias_ref[:, lanes].astype(F32), (8, LANES))
            for c in range(LANES // 32):
                start = first + c * 32
                accs = fir(padded, taps_ref, (h, h), start + HALO - K + 1, range(K), 4, bias)
                for a in range(4):
                    conv_ref[pl.ds(pl.multiple_of(start + 8 * a, 8), 8), lanes] = accs[a]
        total = square = None
        for h in range(lane_blocks):
            conv = conv_ref[here, h * LANES : (h + 1) * LANES]
            total = conv if total is None else total + conv
            square = conv * conv if square is None else square + conv * conv
        row = block * chunks + i
        sums_ref[0, pl.ds(row, 1), :] = lane_sums(total)
        sums_ref[1, pl.ds(row, 1), :] = lane_sums(square)
        return carry

    lax.fori_loop(0, chunks, chunk, 0)


def middle_kernel(
    blocks, total_chans, conv_ref, grad_ref, own_sums_ref, own_sums_hbm, gain_ref, cot_ref,
    normed_grad_ref, sums_ref, gain_grad_ref, weight_out_ref, stats_ref,
    swished, weight_grad_ref, arrived, send_sems, recv_sems,
):
    step = pl.program_id(0)
    rows, chans = conv_ref.shape
    lane_blocks = chans // LANES
    chunks = rows // LANES
    width = cot_ref.shape[1] // chunks
    now = lax.rem(step, 2)
    before = 1 - now

    @pl.when(step == 0)
    def _():
        peers = range(1, lax.axis_size("tp"))
        greet([("tp", d) for d in peers])
        copies = [
            remote(
                own_sums_hbm, arrived.at[d - 1], send_sems.at[d - 1], recv_sems.at[d - 1], "tp", d
            )
            for d in peers
        ]
        for copy in copies:
            copy.start()
        weight_grad_ref[...] = jnp.zeros_like(weight_grad_ref)
        gain_grad_ref[...] = jnp.zeros_like(gain_grad_ref)
        swished[1] = jnp.zeros(swished.shape[1:], BF16)
        total = own_sums_ref[...]
        for d, copy in zip(peers, copies):
            copy.wait()
            total = total + arrived[d - 1]
        stats_ref[...] = total

    fresh = jnp.where(step < blocks, 1.0, 0.0).astype(F32)
    block = jnp.minimum(step, blocks - 1)

    def chunk(i, carry):
        first = pl.multiple_of(i * LANES, LANES)
        here = pl.ds(first, LANES)
        columns = pl.ds(pl.multiple_of(i * width, width), width)
        weight_grad_ref[:, columns] += jnp.dot(
            swished[before], cot_ref[:, columns], preferred_element_type=F32
        )
        row = block * chunks + i
        mean = stats_ref[0, pl.ds(row, 1), :] / total_chans
        variance = stats_ref[1, pl.ds(row, 1), :] / total_chans - mean * mean
        inverse = row_spread(lax.rsqrt(variance + EPS))
        mean = row_spread(mean)
        plain = weighted = None
        for h in range(lane_blocks):
            lanes = slice(h * LANES, (h + 1) * LANES)
            gain = gain_ref[:, lanes]
            normed = (conv_ref[here, lanes] - mean) * inverse
            scaled = normed * gain
            sig = sigmoid(scaled)
            silu = scaled * sig
            swished[now, lanes, here] = silu.T.astype(BF16)
            scaled_grad = grad_ref[here, lanes] * (sig + silu * (1.0 - sig))
            normed_grad = scaled_grad * gain
            normed_grad_ref[here, lanes] = normed_grad
            product = scaled_grad * normed
            gain_grad_ref[:, lanes] += fresh * jnp.sum(
                product.reshape(LANES // 8, 8, LANES), axis=0
            )
            product = product * gain
            plain = normed_grad if plain is None else plain + normed_grad
            weighted = product if weighted is None else weighted + product
        sums_ref[0, pl.ds(row, 1), :] = lane_sums(plain)
        sums_ref[1, pl.ds(row, 1), :] = lane_sums(weighted)
        return carry

    lax.fori_loop(0, chunks, chunk, 0)

    @pl.when(step == blocks)
    def _():
        weight_out_ref[...] = weight_grad_ref[...].astype(BF16)


def backward_kernel(
    total_chans, seqs, values_hbm, gates_hbm, conv_hbm, normed_grad_hbm, weight_hbm, back_hbm,
    halo_ref, taps_ref, stats_ref, own_back_ref, gain_grad_ref,
    values_grad_hbm, gates_grad_hbm, taps_grad_ref, gain_out_ref, bias_out_ref, weight_grad_ref,
    values, gates, conv, normed_grad, padded, wide, heads, back, back_arrived, small,
    small_arrived, own_weight, pair_arrived, weight_arrived, local_sems, out_sems, weight_sem,
    pair_send, pair_recv,
    back_send, back_recv, weight_send, weight_recv, head_send, head_recv, small_send, small_recv,
):
    positions, chans = values.shape
    tokens = positions // seqs
    lane_blocks = chans // LANES
    chunks = tokens // LANES
    sp_devices = lax.axis_size("sp")
    me = lax.axis_index("sp")
    tp_peers = range(1, lax.axis_size("tp"))
    sp_peers = range(1, sp_devices)

    def rows_of(s):
        return pl.ds(s * tokens, tokens)

    loads = []
    for s in range(seqs):
        pairs = ((values_hbm, values), (gates_hbm, gates), (conv_hbm, conv),
                 (normed_grad_hbm, normed_grad))
        loads.append([
            pltpu.make_async_copy(src.at[rows_of(s)], dst.at[rows_of(s)], local_sems.at[s, n])
            for n, (src, dst) in enumerate(pairs)
        ])
        for copy in loads[s]:
            copy.start()
    greet([("tp", d) for d in tp_peers] + [("sp", d) for d in sp_peers])
    back_copies = [
        remote(back_hbm, back_arrived.at[d - 1], back_send.at[d - 1], back_recv.at[d - 1], "tp", d)
        for d in tp_peers
    ]
    for copy in back_copies:
        copy.start()
    group = PAIR if sp_devices % PAIR == 0 else 1
    groups = sp_devices // group
    inner = lax.rem(me, group)
    outer = me // group
    order = list(range(1, groups)) + [0]
    pair_copies, own_copies, weight_copies = {}, {}, {}
    for d in order:
        base = lax.rem(outer + d, groups) * group
        own_copies[d] = pltpu.make_async_copy(
            weight_hbm.at[base + inner], own_weight.at[d], weight_sem.at[d]
        )
        own_copies[d].start()
        if group > 1:
            pair_copies[d] = remote(
                weight_hbm.at[base + 1 - inner], pair_arrived.at[d], pair_send.at[d],
                pair_recv.at[d], "sp", sp_devices + 1 - 2 * inner,
            )
            pair_copies[d].start()
        if d > 0:
            weight_copies[d] = remote(
                own_weight.at[d], weight_arrived.at[d - 1], weight_send.at[d - 1],
                weight_recv.at[d - 1], "sp", d * group,
            )

    def pair_sum(d):
        own_copies[d].wait()
        total = own_weight[d].astype(F32)
        if group > 1:
            pair_copies[d].wait()
            total = total + pair_arrived[d].astype(F32)
        return total

    slots = seqs * lane_blocks + seqs
    todo = {}
    for n, d in enumerate(order[:-1]):
        at = min(n * slots // (2 * groups), slots - 2)
        todo.setdefault(at, []).append((True, d))
        todo.setdefault(at + 1, []).append((False, d))
    slot = [0]

    def forward_slices():
        for adds, d in todo.pop(slot[0], []):
            if adds:
                own_weight[d] = pair_sum(d).astype(BF16)
            else:
                weight_copies[d].start()
        slot[0] += 1

    total = own_back_ref[...]
    for d, copy in zip(tp_peers, back_copies):
        copy.wait()
        total = total + back_arrived[d - 1]
    back[...] = total

    for s in range(seqs):
        for h in range(lane_blocks):
            padded[s * lane_blocks + h, :HALO, :] = halo_ref[s, :, h * LANES : (h + 1) * LANES]
    bias_accs = tuple(jnp.zeros((8, LANES), F32) for _ in range(lane_blocks))
    for s in range(seqs):
        for copy in loads[s]:
            copy.wait()

        def prepare(i, accs):
            accs = list(accs)
            first = pl.multiple_of(i * LANES, LANES)
            here = pl.ds(s * tokens + first, LANES)
            row = s * chunks + i
            mean = stats_ref[0, pl.ds(row, 1), :] / total_chans
            variance = stats_ref[1, pl.ds(row, 1), :] / total_chans - mean * mean
            inverse = row_spread(lax.rsqrt(variance + EPS))
            mean = row_spread(mean)
            plain = row_spread(back[0, pl.ds(row, 1), :] / total_chans)
            weighted = row_spread(back[1, pl.ds(row, 1), :] / total_chans)
            for h in range(lane_blocks):
                lanes = slice(h * LANES, (h + 1) * LANES)
                sig = sigmoid(gates[here, lanes].astype(F32))
                gated = (values[here, lanes].astype(F32) * sig).astype(BF16).astype(F32)
                padded[s * lane_blocks + h, pl.ds(first + HALO, LANES), :] = gated
                normed = (conv[here, lanes] - mean) * inverse
                conv_grad = inverse * (normed_grad[here, lanes] - plain - normed * weighted)
                wide[s * lane_blocks + h, pl.ds(first, LANES), :] = conv_grad
                accs[h] = accs[h] + jnp.sum(conv_grad.reshape(LANES // 8, 8, LANES), axis=0)
            return tuple(accs)

        bias_accs = lax.fori_loop(0, chunks, prepare, bias_accs)

    head_copy = remote(
        wide.at[:, pl.ds(0, HALO)], heads, head_send, head_recv, "sp", sp_devices - 1
    )
    head_copy.start()

    for h in range(lane_blocks):
        accs = tuple(jnp.zeros((8, LANES), F32) for _ in range(K))
        for s in range(seqs):
            where = s * lane_blocks + h

            def correlate(i, accs):
                start = pl.multiple_of(i * 32, 32)
                accs = list(accs)
                grads = [
                    wide[where, pl.ds(pl.multiple_of(start + 8 * a, 8), 8), :] for a in range(4)
                ]
                for offset in range(K + 24):
                    piece = padded[where, pl.ds(start + HALO - K + 1 + offset, 8), :]
                    for a in range(4):
                        k = offset - 8 * a
                        if 0 <= k < K:
                            accs[k] = accs[k] + grads[a] * piece
                return tuple(accs)

            accs = lax.fori_loop(0, tokens // 32, correlate, accs)
            forward_slices()
        lanes = slice(h * LANES, (h + 1) * LANES)
        for k in range(K):
            small[k : k + 1, lanes] = jnp.sum(accs[k], axis=0, keepdims=True)
        small[K : K + 1, lanes] = jnp.sum(bias_accs[h], axis=0, keepdims=True)
        small[K + 1 : K + 2, lanes] = jnp.sum(gain_grad_ref[:, lanes], axis=0, keepdims=True)
        small[K + 2 :, lanes] = jnp.zeros((small.shape[0] - K - 2, LANES), F32)

    small_copies = [
        remote(small, small_arrived.at[d - 1], small_send.at[d - 1], small_recv.at[d - 1], "sp", d)
        for d in sp_peers
    ]

    def spread_chunk(s, start):
        here = pl.ds(pl.multiple_of(s * tokens + start, 32), 32)
        for h in range(lane_blocks):
            lanes = slice(h * LANES, (h + 1) * LANES)
            accs = fir(
                wide, taps_ref, (s * lane_blocks + h, h), start, range(K - 1, -1, -1), 4, None
            )
            gated_grad = jnp.concatenate(accs, axis=0)
            sig = sigmoid(gates[here, lanes].astype(F32))
            values_part = gated_grad * sig
            gates_part = values_part * values[here, lanes].astype(F32) * (1.0 - sig)
            values[here, lanes] = values_part.astype(BF16)
            gates[here, lanes] = gates_part.astype(BF16)

    for s in range(seqs):

        def spread(i, carry):
            spread_chunk(s, pl.multiple_of(i * 32, 32))
            return carry

        lax.fori_loop(0, tokens // 32 - 1, spread, 0)
        forward_slices()
        if s == 0:
            for copy in small_copies:
                copy.start()

    while todo:
        forward_slices()
    head_copy.wait()
    keep = jnp.where(me < sp_devices - 1, 1.0, 0.0).astype(F32)
    stores = []
    for s in range(seqs):
        for h in range(lane_blocks):
            where = s * lane_blocks + h
            wide[where, tokens:, :] = heads[where] * keep
        spread_chunk(s, tokens - 32)
        for n, (src, dst) in enumerate(((values, values_grad_hbm), (gates, gates_grad_hbm))):
            copy = pltpu.make_async_copy(
                src.at[rows_of(s)], dst.at[rows_of(s)], out_sems.at[s, n]
            )
            copy.start()
            stores.append(copy)

    weight_grad_ref[...] = pair_sum(0)
    for d, copy in weight_copies.items():
        copy.wait()
        weight_grad_ref[...] += weight_arrived[d - 1].astype(F32)
    sum_small = small[...]
    for d, copy in zip(sp_peers, small_copies):
        copy.wait()
        sum_small = sum_small + small_arrived[d - 1]
    taps_grad_ref[...] = sum_small[:K]
    bias_out_ref[...] = sum_small[K : K + 1]
    gain_out_ref[...] = sum_small[K + 1 : K + 2]
    for copy in stores:
        copy.wait()


def whole(shape):
    return pl.BlockSpec(shape, lambda i: (0,) * len(shape))


def on_device(values_in, gates_in, conv_taps, conv_bias, norm_gain, out_weight, out_grad):
    seqs, tokens, chans = values_in.shape
    width = out_grad.shape[2]
    total_chans = chans * lax.axis_size("tp")
    lane_blocks = chans // LANES
    positions = seqs * tokens
    rows = min(512, tokens)
    blocks = positions // rows
    stat_rows = positions // LANES

    values = values_in.reshape(positions, chans)
    gates = gates_in.reshape(positions, chans)
    cot = out_grad.reshape(positions, width)

    gain = norm_gain.astype(F32)[None]

    tp_others = lax.axis_size("tp") - 1
    sp_devices = lax.axis_size("sp")
    sp_others = sp_devices - 1

    def params(ident):
        return pltpu.CompilerParams(
            dimension_semantics=("arbitrary",), vmem_limit_bytes=VMEM_LIMIT,
            collective_id=ident, has_side_effects=True,
        )

    def dma(*shape):
        return pltpu.SemaphoreType.DMA(shape)

    anywhere = pl.BlockSpec(memory_space=pl.ANY)
    stats_shape = (2, stat_rows, LANES)
    taps_shape = (lane_blocks, K, 8, LANES)
    seq_blocks = tokens // rows

    def block_of(i):
        return i % seqs * seq_blocks + seq_blocks - 1 - i // seqs

    tile = pl.BlockSpec((rows, chans), lambda i: (block_of(i), 0))
    ahead_halo = pl.BlockSpec(
        (HALO, chans), lambda i: (jnp.maximum(block_of(i) * (rows // HALO) - 1, 0), 0)
    )
    conv, swish_grad, sums, halo, taps8 = pl.pallas_call(
        functools.partial(forward_kernel, seqs, seq_blocks),
        grid=(blocks,),
        in_specs=[
            tile, tile, ahead_halo, ahead_halo, anywhere, anywhere,
            whole(conv_taps.shape),
            whole((1, chans)),
            pl.BlockSpec((rows, width), lambda i: (block_of(i), 0)),
            whole(out_weight.shape),
        ],
        out_specs=[tile, tile, whole(stats_shape), whole((seqs, HALO, chans)),
                   whole(taps_shape)],
        out_shape=[
            jax.ShapeDtypeStruct((positions, chans), F32),
            jax.ShapeDtypeStruct((positions, chans), F32),
            jax.ShapeDtypeStruct(stats_shape, F32),
            jax.ShapeDtypeStruct((seqs, HALO, chans), F32),
            jax.ShapeDtypeStruct(taps_shape, F32),
        ],
        scratch_shapes=[
            pltpu.VMEM((lane_blocks, rows + HALO, LANES), F32),
            pltpu.VMEM((seqs, HALO, chans), BF16),
            pltpu.VMEM((seqs, HALO, chans), BF16),
            dma(2),
            dma(2),
        ],
        compiler_params=params(0),
        name="forward",
    )(values, gates, values, gates, values_in, gates_in, conv_taps,
      conv_bias[None], cot, out_weight)

    ahead = pl.BlockSpec((rows, chans), lambda i: (jnp.minimum(i, blocks - 1), 0))
    normed_grad, back, gain_local, weight_local, stats = pl.pallas_call(
        functools.partial(middle_kernel, blocks, total_chans),
        grid=(blocks + 1,),
        in_specs=[
            ahead,
            ahead,
            whole(stats_shape),
            anywhere,
            whole((1, chans)),
            pl.BlockSpec((rows, width), lambda i: (jnp.maximum(i - 1, 0), 0)),
        ],
        out_specs=[
            ahead,
            whole(stats_shape),
            whole((8, chans)),
            whole((chans, width)),
            whole(stats_shape),
        ],
        out_shape=[
            jax.ShapeDtypeStruct((positions, chans), F32),
            jax.ShapeDtypeStruct(stats_shape, F32),
            jax.ShapeDtypeStruct((8, chans), F32),
            jax.ShapeDtypeStruct((chans, width), BF16),
            jax.ShapeDtypeStruct(stats_shape, F32),
        ],
        scratch_shapes=[
            pltpu.VMEM((2, chans, rows), BF16),
            pltpu.VMEM((chans, width), F32),
            pltpu.VMEM((tp_others, *stats_shape), F32),
            dma(tp_others),
            dma(tp_others),
        ],
        compiler_params=params(1),
        name="middle",
    )(conv, swish_grad, sums, sums, gain, cot)

    small_rows = -(-(K + 2) // 8) * 8
    weight_rows = chans // sp_devices
    groups = sp_devices // PAIR if sp_devices % PAIR == 0 else sp_devices
    padded_shape = (seqs * lane_blocks, tokens + HALO, LANES)
    values_grad, gates_grad, taps_grad, gain_grad, bias_grad, weight_grad = pl.pallas_call(
        functools.partial(backward_kernel, total_chans, seqs),
        in_specs=[anywhere] * 6 + [pl.BlockSpec(memory_space=pltpu.VMEM)] * 5,
        out_specs=[anywhere] * 2 + [pl.BlockSpec(memory_space=pltpu.VMEM)] * 4,
        out_shape=[
            jax.ShapeDtypeStruct((positions, chans), BF16),
            jax.ShapeDtypeStruct((positions, chans), BF16),
            jax.ShapeDtypeStruct((K, chans), F32),
            jax.ShapeDtypeStruct((1, chans), F32),
            jax.ShapeDtypeStruct((1, chans), F32),
            jax.ShapeDtypeStruct((weight_rows, width), F32),
        ],
        scratch_shapes=[
            pltpu.VMEM((positions, chans), BF16),
            pltpu.VMEM((positions, chans), BF16),
            pltpu.VMEM((positions, chans), F32),
            pltpu.VMEM((positions, chans), F32),
            pltpu.VMEM(padded_shape, F32),
            pltpu.VMEM(padded_shape, F32),
            pltpu.VMEM((seqs * lane_blocks, HALO, LANES), F32),
            pltpu.VMEM(stats_shape, F32),
            pltpu.VMEM((tp_others, *stats_shape), F32),
            pltpu.VMEM((small_rows, chans), F32),
            pltpu.VMEM((sp_others, small_rows, chans), F32),
            pltpu.VMEM((groups, weight_rows, width), BF16),
            pltpu.VMEM((groups, weight_rows, width), BF16),
            pltpu.VMEM((max(groups - 1, 1), weight_rows, width), BF16),
            dma(seqs, 4),
            dma(seqs, 2),
            dma(groups),
            dma(groups),
            dma(groups),
            dma(tp_others),
            dma(tp_others),
            dma(max(groups - 1, 1)),
            dma(max(groups - 1, 1)),
            pltpu.SemaphoreType.DMA,
            pltpu.SemaphoreType.DMA,
            dma(sp_others),
            dma(sp_others),
        ],
        compiler_params=pltpu.CompilerParams(
            vmem_limit_bytes=VMEM_LIMIT, collective_id=2, has_side_effects=True
        ),
        name="backward",
    )(
        values, gates, conv, normed_grad,
        weight_local.reshape(sp_devices, weight_rows, width), back,
        halo, taps8, stats, back, gain_local,
    )
    return (
        values_grad.reshape(values_in.shape),
        gates_grad.reshape(values_in.shape),
        taps_grad,
        gain_grad[0],
        bias_grad[0],
        weight_grad,
    )


def solution(mesh):
    return jax.shard_map(
        on_device,
        mesh=mesh,
        in_specs=(
            P(None, "sp", "tp"),
            P(None, "sp", "tp"),
            P(None, "tp"),
            P("tp"),
            P("tp"),
            P("tp", None),
            P(None, "sp", None),
        ),
        out_specs=(
            P(None, "sp", "tp"),
            P(None, "sp", "tp"),
            P(None, "tp"),
            P("tp"),
            P("tp"),
            P(("tp", "sp"), None),
        ),
        check_vma=False,
    )
```

profile of v0, /device:TPU:0, one launch (start us, length us, event | category | flops | bytes accessed | tf_op | source)
XLA Modules:
  0.0 119.5 jit_solution(2764519813347625336)
XLA Ops:
  0.6 1.2 %broadcast_in_dim.8.bias_ref = bf16[1,256]{1,0:T(2,128)(2,1)} reshape(bf16[256]{0:T(256)(128)(2,1)} %param.10) | data formatting | bytes 1024 | tf_op jit(solution)/shard_map/broadcast_in_dim | solution.py:531
  1.9 1.2 %broadcast_in_dim.11 = f32[256]{0:T(256)} convert(bf16[256]{0:T(256)(128)(2,1)} %param.11) | non-fusion elementwise | flops 256 | bytes 1536 | tf_op jit(solution)/shard_map/broadcast_in_dim | solution.py:475
  3.1 33.8 %forward.1 = (f32[4096,256]{1,0:T(8,128)}, f32[4096,256]{1,0:T(8,128)}, f32[2,32,128]{2,1,0:T(8,128)}, f32[4,32,256]{2,1,0:T(8,128)}, f32[2,31,8,128]{3,2,1,0:T(8,128)}) custom-call(bf16[4096,256]{1,0:T(8,128)(2,1)} %bitcast.11, bf16[4096,256]{1,0:T(8,128)(2,1)} %bitcast.14, bf16[4096,256]{1,0:T(8,128)(2,1)} %bitcast.12, bf16[4096,256]{1,0:T(8,128)(2,1)} %bitcast.15, ...), custom_call_target="tpu_custom_call" | custom-call | tf_op jit(solution)/shard_map/forward/pallas_call | solution.py:502
  36.9 28.5 %middle.1 = (f32[4096,256]{1,0:T(8,128)}, f32[2,32,128]{2,1,0:T(8,128)}, f32[8,256]{1,0:T(8,128)}, bf16[256,4096]{1,0:T(8,128)(2,1)}, f32[2,32,128]{2,1,0:T(8,128)}) custom-call(f32[4096,256]{1,0:T(8,128)} %get-tuple-element.22.conv_ref.conv_hbm, f32[4096,256]{1,0:T(8,128)} %get-tuple-element.23.grad_ref, ...), custom_call_target="tpu_custom_call" | custom-call | tf_op jit(solution)/shard_map/middle/pallas_call | solution.py:534
  65.5 46.9 %backward.1 = (bf16[4096,256]{1,0:T(8,128)(2,1)}, bf16[4096,256]{1,0:T(8,128)(2,1)}, f32[31,256]{1,0:T(8,128)}, f32[1,256]{1,0:T(1,128)}, f32[1,256]{1,0:T(1,128)}, /*index=5*/f32[32,4096]{1,0:T(8,128)}) custom-call(bf16[4096,256]{1,0:T(8,128)(2,1)} %bitcast.13, bf16[4096,256]{1,0:T(8,128)(2,1)} %bitcast.16, ...), custom_call_target="tpu_custom_call" | custom-call | tf_op jit(solution)/shard_map/backward/pallas_call | solution.py:574
  112.4 0.0 copy-start
  112.4 3.2 %copy.19 = bf16[4,1024,256]{2,1,0:T(8,128)(2,1)} copy(bf16[4,1024,256]{2,1,0:T(8,128)(2,1)} %bitcast.18) | data formatting | bytes 4194304
  115.6 0.0 copy-done
  115.6 0.0 copy-start.2
  115.6 0.0 copy-start.4
  115.6 0.0 copy-start.3
  115.6 0.0 copy-start.1
  115.6 1.3 %copy.20 = bf16[4,1024,256]{2,1,0:T(8,128)(2,1)} copy(bf16[4,1024,256]{2,1,0:T(8,128)(2,1)S(1)} %bitcast.17) | data formatting | bytes 4194304
  116.9 0.0 copy-done.2
  116.9 0.6 copy.21
  117.6 0.0 copy-done.4
  117.6 0.6 copy.22
  118.1 0.0 copy-done.3
  118.1 0.6 copy.23
  118.7 0.0 copy-done.1
  118.7 0.8 copy.24
Async XLA Ops:
  112.4 3.2 %copy-start = (bf16[4096,256]{1,0:T(8,128)(2,1)S(1)}, bf16[4096,256]{1,0:T(8,128)(2,1)}, u32[]{:S(2)}) copy-start(bf16[4096,256]{1,0:T(8,128)(2,1)} %get-tuple-element.33) | copy-start | bytes 6291460
  115.6 1.3 %copy-start.2 = (f32[31,256]{1,0:T(8,128)S(1)}, f32[31,256]{1,0:T(8,128)}, u32[]{:S(2)}) copy-start(f32[31,256]{1,0:T(8,128)} %get-tuple-element.46) | copy-start | bytes 95236
  115.6 2.0 %copy-start.4 = (f32[1,256]{1,0:T(1,128)S(1)}, f32[1,256]{1,0:T(1,128)}, u32[]{:S(2)}) copy-start(f32[1,256]{1,0:T(1,128)} %get-tuple-element.35) | copy-start | bytes 3076
  115.6 2.5 %copy-start.3 = (f32[1,256]{1,0:T(1,128)S(1)}, f32[1,256]{1,0:T(1,128)}, u32[]{:S(2)}) copy-start(f32[1,256]{1,0:T(1,128)} %get-tuple-element.36) | copy-start | bytes 3076
  115.6 3.1 %copy-start.1 = (f32[32,4096]{1,0:T(8,128)S(1)}, f32[32,4096]{1,0:T(8,128)}, u32[]{:S(2)}) copy-start(f32[32,4096]{1,0:T(8,128)} %get-tuple-element.49) | copy-start | bytes 1572868
where the time goes:
time: 120 us; the launch traced here: 119 us
  Pallas kernels  109 us (91%)
  local copies, waits for them, and re-layouts  8.29 us (7%)
  other arithmetic  1.22 us (1%)
    pallas_call x1, Pallas kernels, on_device(): pl.pallas_call(functools.partial(backward_kernel, total_chans, seqs), in_...  46.9 us
    pallas_call x1, Pallas kernels, on_device(): pl.pallas_call(functools.partial(forward_kernel, seqs, seq_blocks), grid=...  33.8 us
    pallas_call x1, Pallas kernels, on_device(): pl.pallas_call(functools.partial(middle_kernel, blocks, total_chans), gri...  28.5 us
    unnamed x16, local copies, waits for them, and re-layouts  7.07 us

commit v1 on v0

v1 whole, which is shorter than its diff:
```python
import functools

import jax
import jax.numpy as jnp
import numpy as np
from jax import lax
from jax.experimental import pallas as pl
from jax.experimental.pallas import tpu as pltpu
from jax.sharding import PartitionSpec as P

K = 31
EPS = 1e-05
HALO = 32
PAIR = 2
LANES = 128
SPAN = 256
STEP = SPAN - HALO
F32 = jnp.float32
BF16 = jnp.bfloat16
VMEM_LIMIT = 64 * 1024 * 1024 - 64 * 1024

FWD, GRAD, INV, CONV, TAPF, TAPI = 0, 512, 1024, 1536, 1984, 2496
TABLE_ROWS = 2560


def transform_table():
    row = np.arange(SPAN)
    freq = 8 * (row // 16) + row % 8
    angle = 2 * np.pi * (freq[:, None] + 0.5) * np.arange(SPAN)[None] / SPAN
    fwd = np.where((row // 8 % 2 == 0)[:, None], np.cos(angle), -np.sin(angle))
    inv = fwd.T * (2 / SPAN)
    grad = np.zeros((SPAN, SPAN))
    grad[:, :STEP] = fwd[:, HALO:]
    tap_fwd = np.zeros((SPAN, SPAN))
    tap_fwd[:, :K] = fwd[:, K - 1 :: -1]
    tap_inv = np.zeros((32, SPAN))
    tap_inv[:K] = inv[K - 1 :: -1]
    parts = []
    for whole_part in (fwd, grad, inv, inv[HALO:], tap_fwd, tap_inv):
        high = whole_part.astype(BF16)
        parts += [high, (whole_part - high.astype(np.float64)).astype(BF16)]
    return np.concatenate(parts)


def sigmoid(x):
    return 0.5 * jnp.tanh(0.5 * x) + 0.5


def peer_id(axis, distance):
    devices = lax.axis_size(axis)
    return {axis: lax.rem(lax.axis_index(axis) + distance, devices)}


def greet(pairs):
    barrier = pltpu.get_barrier_semaphore()
    for axis, distance in pairs:
        pl.semaphore_signal(
            barrier, inc=1, device_id=peer_id(axis, distance),
            device_id_type=pl.DeviceIdType.MESH,
        )
    pl.semaphore_wait(barrier, len(pairs))


def remote(src, dst, send_sem, recv_sem, axis, distance):
    return pltpu.make_async_remote_copy(
        src_ref=src, dst_ref=dst, send_sem=send_sem, recv_sem=recv_sem,
        device_id=peer_id(axis, distance), device_id_type=pl.DeviceIdType.MESH,
    )


def dot(a, b):
    return jnp.dot(a, b, preferred_element_type=F32)


def lane_sums(x):
    return jnp.sum(x.T, axis=0, keepdims=True)


def row_spread(row):
    return jnp.broadcast_to(row, (LANES, LANES)).T


def split(x):
    high = x.astype(BF16)
    return high, (x - high.astype(F32)).astype(BF16)


def fused_kernel(
    total_chans, values_hbm, gates_hbm, cot_hbm, weight_hbm, table_hbm, taps_ref, bias_ref,
    gain_ref,
    spread_hbm, heads_ref, small_ref, weight_out_ref,
    values, gates, values_halo, gates_halo, cot, swished, weight_t, weight_grad, pair, onward,
    arrived, conv, grad, xpad, spectrum, high, low, grad_high, grad_low, table, tap_rows,
    tap_re, tap_im, corr_re, corr_im, heads, heads_in, sums, sums_in, stat, back, back_in,
    gain_acc, bias_acc, small, small_in,
    load_sems, cot_sems, misc_sems, out_sems, halo_send, halo_recv, sums_send, sums_recv,
    back_send, back_recv, pair_send, pair_recv, onward_send, onward_recv, head_send, head_recv,
    small_send, small_recv,
):
    seqs, tokens, chans = values.shape
    positions, width = cot.shape
    lane_blocks = chans // LANES
    chunks = tokens // LANES
    windows = spectrum.shape[0] // seqs
    blocks, rows = cot_sems.shape[0], grad.shape[1]
    seq_blocks = blocks // seqs
    block_chunks = rows // LANES
    parts = pair_send.shape[0]
    part_width = width // parts
    groups, weight_rows = pair.shape[0], pair.shape[1]
    sp_devices = lax.axis_size("sp")
    me = lax.axis_index("sp")
    inner = lax.rem(me, PAIR)
    outer = me // PAIR
    tp_peers = range(1, lax.axis_size("tp"))
    sp_peers = range(1, sp_devices)

    loads = []
    for n, (src, dst) in enumerate(((weight_hbm, swished.at[:, :width]), (table_hbm, table))):
        copy = pltpu.make_async_copy(src, dst, misc_sems.at[n])
        copy.start()
        loads.append(copy)

    def seq_loads(s):
        return [
            pltpu.make_async_copy(src.at[s], dst.at[s], load_sems.at[n, s])
            for n, (src, dst) in enumerate(((values_hbm, values), (gates_hbm, gates)))
        ]

    for s in range(seqs):
        for copy in seq_loads(s):
            copy.start()

    def cot_load(i):
        here = pl.ds(pl.multiple_of(i * rows, rows), rows)
        return pltpu.make_async_copy(cot_hbm.at[here], cot.at[here], cot_sems.at[i])

    for i in range(blocks):
        cot_load(i).start()

    greet([("tp", d) for d in tp_peers] + [("sp", d) for d in sp_peers])
    last = pl.ds(tokens - HALO, HALO)
    halo_copies = [
        remote(src.at[:, last], dst, halo_send.at[n], halo_recv.at[n], "sp", 1)
        for n, (src, dst) in enumerate(((values_hbm, values_halo), (gates_hbm, gates_halo)))
    ]
    for copy in halo_copies:
        copy.start()

    xpad[HALO + tokens :, :] = jnp.zeros((xpad.shape[0] - HALO - tokens, chans), BF16)
    for ref in (grad_high, grad_low):
        ref[tokens:, :] = jnp.zeros((ref.shape[0] - tokens, chans), BF16)
    for ref in (gain_acc, bias_acc, corr_re, corr_im, tap_rows):
        ref[...] = jnp.zeros_like(ref)
    tap_rows[:K, :] = taps_ref[...].astype(F32)
    bias = bias_ref[...].astype(F32).reshape(1, chans)
    gain = gain_ref[...].astype(F32).reshape(1, chans)

    for copy in loads:
        copy.wait()
    taps_wide = dot(table[TAPF : TAPF + 2 * SPAN], tap_rows[...].astype(BF16))
    taps_wide = taps_wide[:SPAN] + taps_wide[SPAN:]
    for q in range(SPAN // 16):
        tap_re[8 * q : 8 * q + 8, :] = taps_wide[16 * q : 16 * q + 8]
        tap_im[8 * q : 8 * q + 8, :] = taps_wide[16 * q + 8 : 16 * q + 16]

    def turn(i, carry):
        here = pl.ds(pl.multiple_of(i * 512, 512), 512)
        weight_t[here, :] = swished[:, here].T
        return carry

    lax.fori_loop(0, width // 512, turn, 0)

    def product(x, w, sign):
        for q in range(SPAN // 16):
            a, b = tap_re[8 * q : 8 * q + 8, :], tap_im[8 * q : 8 * q + 8, :]
            re, im = x[16 * q : 16 * q + 8], x[16 * q + 8 : 16 * q + 16]
            if sign > 0:
                both = (a * re - b * im, a * im + b * re)
            else:
                both = (a * re + b * im, a * im - b * re)
            here = slice(16 * q, 16 * q + 16)
            high[w, here, :], low[w, here, :] = split(jnp.concatenate(both, axis=0))

    def sums_copies(s):
        return [
            remote(sums.at[s], sums_in.at[d - 1, s], sums_send.at[d - 1, s],
                   sums_recv.at[d - 1, s], "tp", d)
            for d in tp_peers
        ]

    for copy in halo_copies:
        copy.wait()
    keep = jnp.where(me > 0, 1.0, 0.0).astype(F32)

    def gate(values_part, gates_part):
        return values_part.astype(F32) * sigmoid(gates_part.astype(F32))

    def ahead(s, carry):
        for copy in seq_loads(s):
            copy.wait()
        xpad[:HALO, :] = (gate(values_halo[s], gates_halo[s]) * keep).astype(BF16)
        for i in range(chunks):
            here = slice(i * LANES, (i + 1) * LANES)
            xpad[HALO + i * LANES : HALO + (i + 1) * LANES, :] = gate(
                values[s, here, :], gates[s, here, :]
            ).astype(BF16)
        for w in range(windows):
            x = dot(table[FWD : FWD + 2 * SPAN], xpad[w * STEP : w * STEP + SPAN, :])
            x = x[:SPAN] + x[SPAN:]
            spectrum[s * windows + w] = x.astype(BF16)
            product(x, w, 1)
        for w in range(windows):
            y = dot(table[CONV : CONV + 2 * STEP], high[w])
            y = y[:STEP] + y[STEP:] + dot(table[CONV : CONV + STEP], low[w]) + bias
            count = min(STEP, tokens - w * STEP)
            conv[s, w * STEP : w * STEP + count, :] = y[:count]
        for i in range(chunks):
            total = square = None
            for h in range(lane_blocks):
                part = conv[s, i * LANES : (i + 1) * LANES, h * LANES : (h + 1) * LANES]
                total = part if total is None else total + part
                square = part * part if square is None else square + part * part
            sums[s, 0, i : i + 1, :] = lane_sums(total)
            sums[s, 1, i : i + 1, :] = lane_sums(square)
        for copy in sums_copies(s):
            copy.start()
        return carry

    lax.fori_loop(0, seqs, ahead, 0)

    def norm(s, carry):
        total = sums[s]
        for d, copy in zip(tp_peers, sums_copies(s)):
            copy.wait()
            total = total + sums_in[d - 1, s]
        mean_rows = total[0] / total_chans
        variance = total[1] / total_chans - mean_rows * mean_rows
        inverse_rows = lax.rsqrt(variance + EPS)
        stat[s] = inverse_rows
        for i in range(chunks):
            here = slice(i * LANES, (i + 1) * LANES)
            columns = pl.ds(pl.multiple_of(s * tokens + i * LANES, LANES), LANES)
            mean = row_spread(mean_rows[i : i + 1])
            inverse = row_spread(inverse_rows[i : i + 1])
            for h in range(lane_blocks):
                lanes = slice(h * LANES, (h + 1) * LANES)
                normed = (conv[s, here, lanes] - mean) * inverse
                conv[s, here, lanes] = normed
                scaled = normed * gain[:, lanes]
                swished[lanes, columns] = (scaled * sigmoid(scaled)).T.astype(BF16)
        return carry

    lax.fori_loop(0, seqs, norm, 0)

    for i in range(blocks):
        cot_load(i).wait()

    def part_columns(c):
        return pl.ds(pl.multiple_of(c * part_width, part_width), part_width)

    def pair_copy(c):
        columns = part_columns(c)
        return remote(
            weight_grad.at[1 - inner, :, :, columns], pair.at[:, :, columns], pair_send.at[c],
            pair_recv.at[c], "sp", sp_devices + 1 - 2 * inner,
        )

    def onward_copy(d, c):
        columns = part_columns(c)
        return remote(
            onward.at[d - 1, :, columns], arrived.at[d - 1, :, columns], onward_send.at[d - 1, c],
            onward_recv.at[d - 1, c], "sp", d * PAIR,
        )

    def project(c, carry):
        columns = part_columns(c)
        result = dot(swished[:, :positions], cot[:, columns])
        for g in range(groups):
            for n in range(PAIR):
                first = (g * PAIR + n) * weight_rows
                weight_grad[n, g, :, columns] = result[first : first + weight_rows].astype(BF16)
        pair_copy(c).start()
        return carry

    lax.fori_loop(0, parts, project, 0)

    def pass_on(c):
        columns = part_columns(c)
        pair_copy(c).wait()
        for d in range(1, groups):
            target = lax.rem(outer + d, groups)
            onward[d - 1, :, columns] = (
                weight_grad[inner, target, :, columns].astype(F32)
                + pair[target, :, columns].astype(F32)
            ).astype(BF16)
        for d in range(1, groups):
            onward_copy(d, c).start()

    def back_copies(j):
        return [
            remote(back.at[j], back_in.at[d - 1, j], back_send.at[d - 1, j],
                   back_recv.at[d - 1, j], "tp", d)
            for d in tp_peers
        ]

    def multiply(j):
        here = pl.ds(pl.multiple_of(j * rows, rows), rows)
        grad[lax.rem(j, 2)] = dot(cot[here, :], weight_t[...])

    def middle(j):
        s = j // seq_blocks
        first = lax.rem(j, seq_blocks) * rows
        slot = lax.rem(j, 2)
        for i in range(block_chunks):
            here = pl.ds(pl.multiple_of(first + i * LANES, LANES), LANES)
            plain = weighted = None
            for h in range(lane_blocks):
                lanes = slice(h * LANES, (h + 1) * LANES)
                normed = conv[s, here, lanes]
                scaled = normed * gain[:, lanes]
                sig = sigmoid(scaled)
                silu = scaled * sig
                scaled_grad = grad[slot, i * LANES : (i + 1) * LANES, lanes] * (
                    sig + silu * (1.0 - sig)
                )
                normed_grad = scaled_grad * gain[:, lanes]
                values[s, here, lanes], gates[s, here, lanes] = split(normed_grad)
                term = scaled_grad * normed
                gain_acc[:, lanes] += jnp.sum(term.reshape(LANES // 8, 8, LANES), axis=0)
                term = normed_grad * normed
                plain = normed_grad if plain is None else plain + normed_grad
                weighted = term if weighted is None else weighted + term
            back[j, 0, i : i + 1, :] = lane_sums(plain)
            back[j, 1, i : i + 1, :] = lane_sums(weighted)
        for copy in back_copies(j):
            copy.start()

    multiply(0)

    def both(j, carry):
        middle(j - 1)
        multiply(j)

        @pl.when(lax.rem(j, 2) == 0)
        def _():
            pass_on(j // 2 - 1)

        return carry

    lax.fori_loop(1, blocks, both, 0)
    middle(blocks - 1)
    passed = min((blocks - 1) // 2, parts)

    def spread_copy(s):
        return pltpu.make_async_copy(conv.at[s], spread_hbm.at[s], out_sems.at[s])

    def head_copy(s):
        return remote(
            heads.at[s], heads_in.at[s], head_send.at[s], head_recv.at[s], "sp", sp_devices - 1
        )

    def behind(s, carry):
        for n in range(seq_blocks):
            for copy in back_copies(s * seq_blocks + n):
                copy.wait()
        for i in range(chunks):
            here = slice(i * LANES, (i + 1) * LANES)
            j = s * seq_blocks + i // block_chunks
            at = slice(i % block_chunks, i % block_chunks + 1)
            inverse_row = stat[s, i : i + 1, :]
            plain, weighted = back[j, 0, at, :], back[j, 1, at, :]
            for d in tp_peers:
                plain = plain + back_in[d - 1, j, 0, at, :]
                weighted = weighted + back_in[d - 1, j, 1, at, :]
            scale = inverse_row / total_chans
            inverse = row_spread(inverse_row)
            plain = row_spread(plain * scale)
            weighted = row_spread(weighted * scale)
            for h in range(lane_blocks):
                lanes = slice(h * LANES, (h + 1) * LANES)
                normed_grad = values[s, here, lanes].astype(F32) + gates[s, here, lanes].astype(
                    F32
                )
                conv_grad = inverse * normed_grad - plain - conv[s, here, lanes] * weighted
                grad_high[here, lanes], grad_low[here, lanes] = split(conv_grad)
                bias_acc[:, lanes] += jnp.sum(conv_grad.reshape(LANES // 8, 8, LANES), axis=0)
        for w in range(windows):
            here = slice(w * STEP, w * STEP + SPAN)
            g = dot(table[GRAD : GRAD + 2 * SPAN], grad_high[here, :])
            g = g[:SPAN] + g[SPAN:] + dot(table[GRAD : GRAD + SPAN], grad_low[here, :])
            x = spectrum[s * windows + w].astype(F32)
            for q in range(SPAN // 16):
                at = slice(8 * q, 8 * q + 8)
                g_re, g_im = g[16 * q : 16 * q + 8], g[16 * q + 8 : 16 * q + 16]
                x_re, x_im = x[16 * q : 16 * q + 8], x[16 * q + 8 : 16 * q + 16]
                corr_re[at, :] += g_re * x_re + g_im * x_im
                corr_im[at, :] += g_im * x_re - g_re * x_im
            product(g, w, -1)
        for w in range(windows):
            y = dot(table[INV : INV + 2 * SPAN], high[w])
            y = y[:SPAN] + y[SPAN:] + dot(table[INV : INV + SPAN], low[w])
            if w == 0:
                heads[s] = y[:HALO]
            else:
                conv[s, w * STEP - HALO : w * STEP, :] += y[:HALO]
            count = min(STEP, tokens - w * STEP)
            conv[s, w * STEP : w * STEP + count, :] = y[HALO : HALO + count]
        spread_copy(s).start()
        head_copy(s).start()

        @pl.when(passed + s < parts)
        def _():
            pass_on(passed + s)

        return carry

    lax.fori_loop(0, seqs, behind, 0)

    corr = []
    for q in range(SPAN // 16):
        corr += [corr_re[8 * q : 8 * q + 8, :], corr_im[8 * q : 8 * q + 8, :]]
    corr_high, corr_low = split(jnp.concatenate(corr, axis=0))
    taps_grad = dot(table[TAPI : TAPI + 64], corr_high)
    taps_grad = taps_grad[:32] + taps_grad[32:] + dot(table[TAPI : TAPI + 32], corr_low)
    small[:32, :] = taps_grad
    small[32:33, :] = jnp.sum(bias_acc[...], axis=0, keepdims=True)
    small[33:34, :] = jnp.sum(gain_acc[...], axis=0, keepdims=True)
    small[34:, :] = jnp.zeros((small.shape[0] - 34, chans), F32)
    small_copies = [
        remote(small, small_in.at[d - 1], small_send.at[d - 1], small_recv.at[d - 1], "sp", d)
        for d in sp_peers
    ]
    for copy in small_copies:
        copy.start()

    for c in range(min(passed + seqs, parts), parts):
        pass_on(c)

    keep_head = jnp.where(me < sp_devices - 1, 1.0, 0.0).astype(F32)
    for s in range(seqs):
        head_copy(s).wait()
        heads_ref[s] = heads_in[s] * keep_head
    total = small[...]
    for d, copy in zip(sp_peers, small_copies):
        copy.wait()
        total = total + small_in[d - 1]
    small_ref[...] = total
    for c in range(parts):
        columns = slice(c * part_width, (c + 1) * part_width)
        result = weight_grad[inner, outer, :, columns].astype(F32)
        result = result + pair[outer, :, columns].astype(F32)
        for d in range(1, groups):
            onward_copy(d, c).wait()
            result = result + arrived[d - 1, :, columns].astype(F32)
        weight_out_ref[:, columns] = result
    for s in range(seqs):
        spread_copy(s).wait()


def finish_kernel(
    seq_blocks, spread_ref, heads_ref, values_ref, gates_ref, small_ref, weight_ref,
    values_grad_ref, gates_grad_ref, taps_grad_ref, gain_grad_ref, bias_grad_ref, weight_grad_ref,
    gated_grad,
):
    step = pl.program_id(0)
    rows = spread_ref.shape[0]
    share = jnp.where(lax.rem(step, seq_blocks) == seq_blocks - 1, 1.0, 0.0).astype(F32)

    @pl.when(step == 0)
    def _():
        taps_grad_ref[...] = small_ref[:K]
        bias_grad_ref[...] = small_ref[32:33]
        gain_grad_ref[...] = small_ref[33:34]
        weight_grad_ref[...] = weight_ref[...]

    gated_grad[...] = spread_ref[...]
    gated_grad[rows - HALO :, :] += heads_ref[...] * share
    for i in range(rows // LANES):
        here = slice(i * LANES, (i + 1) * LANES)
        sig = sigmoid(gates_ref[here, :].astype(F32))
        values_part = gated_grad[here, :] * sig
        values_grad_ref[here, :] = values_part.astype(BF16)
        gates_part = values_part * values_ref[here, :].astype(F32) * (1.0 - sig)
        gates_grad_ref[here, :] = gates_part.astype(BF16)


def whole(shape):
    return pl.BlockSpec(shape, lambda i: (0,) * len(shape))


def on_device(values_in, gates_in, conv_taps, conv_bias, norm_gain, out_weight, out_grad):
    seqs, tokens, chans = values_in.shape
    width = out_grad.shape[2]
    total_chans = chans * lax.axis_size("tp")
    positions = seqs * tokens
    rows = min(512, tokens)
    blocks = positions // rows
    seq_blocks = tokens // rows
    chunks = tokens // LANES
    windows = -(-tokens // STEP)
    parts = 8
    tp_others = lax.axis_size("tp") - 1
    sp_devices = lax.axis_size("sp")
    sp_others = sp_devices - 1
    groups = sp_devices // PAIR
    weight_rows = chans // sp_devices
    small_rows = 40

    def dma(*shape):
        return pltpu.SemaphoreType.DMA(shape)

    anywhere = pl.BlockSpec(memory_space=pl.ANY)
    vmem = pl.BlockSpec(memory_space=pltpu.VMEM)
    padded = windows * STEP + HALO
    block_sums = (2, rows // LANES, LANES)
    spread, heads, small, weight_sum = pl.pallas_call(
        functools.partial(fused_kernel, total_chans),
        in_specs=[anywhere] * 5 + [vmem] * 3,
        out_specs=[anywhere] + [vmem] * 3,
        out_shape=[
            jax.ShapeDtypeStruct((seqs, tokens, chans), F32),
            jax.ShapeDtypeStruct((seqs, HALO, chans), F32),
            jax.ShapeDtypeStruct((small_rows, chans), F32),
            jax.ShapeDtypeStruct((weight_rows, width), F32),
        ],
        scratch_shapes=[
            pltpu.VMEM((seqs, tokens, chans), BF16),
            pltpu.VMEM((seqs, tokens, chans), BF16),
            pltpu.VMEM((seqs, HALO, chans), BF16),
            pltpu.VMEM((seqs, HALO, chans), BF16),
            pltpu.VMEM((positions, width), BF16),
            pltpu.VMEM((chans, max(positions, width)), BF16),
            pltpu.VMEM((width, chans), BF16),
            pltpu.VMEM((PAIR, groups, weight_rows, width), BF16),
            pltpu.VMEM((groups, weight_rows, width), BF16),
            pltpu.VMEM((groups - 1, weight_rows, width), BF16),
            pltpu.VMEM((groups - 1, weight_rows, width), BF16),
            pltpu.VMEM((seqs, tokens, chans), F32),
            pltpu.VMEM((2, rows, chans), F32),
            pltpu.VMEM((padded, chans), BF16),
            pltpu.VMEM((seqs * windows, SPAN, chans), BF16),
            pltpu.VMEM((windows, SPAN, chans), BF16),
            pltpu.VMEM((windows, SPAN, chans), BF16),
            pltpu.VMEM((padded, chans), BF16),
            pltpu.VMEM((padded, chans), BF16),
            pltpu.VMEM((TABLE_ROWS, SPAN), BF16),
            pltpu.VMEM((SPAN, chans), F32),
            pltpu.VMEM((SPAN // 2, chans), F32),
            pltpu.VMEM((SPAN // 2, chans), F32),
            pltpu.VMEM((SPAN // 2, chans), F32),
            pltpu.VMEM((SPAN // 2, chans), F32),
            pltpu.VMEM((seqs, HALO, chans), F32),
            pltpu.VMEM((seqs, HALO, chans), F32),
            pltpu.VMEM((seqs, 2, chunks, LANES), F32),
            pltpu.VMEM((tp_others, seqs, 2, chunks, LANES), F32),
            pltpu.VMEM((seqs, chunks, LANES), F32),
            pltpu.VMEM((blocks, *block_sums), F32),
            pltpu.VMEM((tp_others, blocks, *block_sums), F32),
            pltpu.VMEM((8, chans), F32),
            pltpu.VMEM((8, chans), F32),
            pltpu.VMEM((small_rows, chans), F32),
            pltpu.VMEM((sp_others, small_rows, chans), F32),
            dma(2, seqs),
            dma(blocks),
            dma(2),
            dma(seqs),
            dma(2),
            dma(2),
            dma(tp_others, seqs),
            dma(tp_others, seqs),
            dma(tp_others, blocks),
            dma(tp_others, blocks),
            dma(parts),
            dma(parts),
            dma(groups - 1, parts),
            dma(groups - 1, parts),
            dma(seqs),
            dma(seqs),
            dma(sp_others),
            dma(sp_others),
        ],
        compiler_params=pltpu.CompilerParams(
            vmem_limit_bytes=VMEM_LIMIT, collective_id=0, has_side_effects=True
        ),
        name="fused",
    )(
        values_in, gates_in, out_grad.reshape(positions, width), out_weight,
        jnp.asarray(transform_table()), conv_taps, conv_bias, norm_gain,
    )

    tile = pl.BlockSpec((rows, chans), lambda i: (i, 0))
    values_grad, gates_grad, taps_grad, gain_grad, bias_grad, weight_grad = pl.pallas_call(
        functools.partial(finish_kernel, seq_blocks),
        grid=(blocks,),
        in_specs=[
            tile, pl.BlockSpec((HALO, chans), lambda i: (i // seq_blocks, 0)), tile, tile,
            whole((small_rows, chans)), whole((weight_rows, width)),
        ],
        out_specs=[
            tile, tile, whole((K, chans)), whole((1, chans)), whole((1, chans)),
            whole((weight_rows, width)),
        ],
        out_shape=[
            jax.ShapeDtypeStruct((positions, chans), BF16),
            jax.ShapeDtypeStruct((positions, chans), BF16),
            jax.ShapeDtypeStruct((K, chans), F32),
            jax.ShapeDtypeStruct((1, chans), F32),
            jax.ShapeDtypeStruct((1, chans), F32),
            jax.ShapeDtypeStruct((weight_rows, width), F32),
        ],
        scratch_shapes=[pltpu.VMEM((rows, chans), F32)],
        compiler_params=pltpu.CompilerParams(dimension_semantics=("arbitrary",)),
        name="finish",
    )(
        spread.reshape(positions, chans), heads.reshape(seqs * HALO, chans),
        values_in.reshape(positions, chans), gates_in.reshape(positions, chans),
        small, weight_sum,
    )
    return (
        values_grad.reshape(values_in.shape),
        gates_grad.reshape(values_in.shape),
        taps_grad,
        gain_grad[0],
        bias_grad[0],
        weight_grad,
    )


def solution(mesh):
    return jax.shard_map(
        on_device,
        mesh=mesh,
        in_specs=(
            P(None, "sp", "tp"),
            P(None, "sp", "tp"),
            P(None, "tp"),
            P("tp"),
            P("tp"),
            P("tp", None),
            P(None, "sp", None),
        ),
        out_specs=(
            P(None, "sp", "tp"),
            P(None, "sp", "tp"),
            P(None, "tp"),
            P("tp"),
            P("tp"),
            P(("tp", "sp"), None),
        ),
        check_vma=False,
    )
```

time: 120 us -> 88.1 us (0.73)
  Pallas kernels: 109 us -> 87.1 us
  local copies, waits for them, and re-layouts: 8.29 us -> 0 us
  other arithmetic: 1.22 us -> 0 us
    pallas_call x3 -> x2, Pallas kernels: 109 us -> 87.1 us  [the longest x1 78.8 us: on_device(): pl.pallas_call(functools.partial(fused_kernel, total_chans), in_specs=[an...]
    unnamed x16 -> x0, local copies, waits for them, and re-layouts: 7.07 us -> none
    broadcast_in_dim x1 -> x0, local copies, waits for them, and re-layouts: 1.22 us -> none  [on_device(): conv_bias[None]]
    broadcast_in_dim x1 -> x0, other arithmetic: 1.22 us -> none  [on_device(): gain = norm_gain.astype(F32)[None]]
where the time goes in v1:
time: 88.1 us; the launch traced here: 87.8 us
  Pallas kernels  87.1 us (99%)
    pallas_call x1, Pallas kernels, on_device(): pl.pallas_call(functools.partial(fused_kernel, total_chans), in_specs=[an...  78.8 us
    pallas_call x1, Pallas kernels, on_device(): pl.pallas_call(functools.partial(finish_kernel, seq_blocks), grid=(blocks...  8.31 us

profile of v1, /device:TPU:0, one launch (start us, length us, event | category | flops | bytes accessed | tf_op | source)
XLA Modules:
  0.0 87.8 jit_solution(8127347633909381065)
XLA Ops:
  0.6 78.8 %fused.1 = (f32[4,1024,256]{2,1,0:T(8,128)}, f32[4,32,256]{2,1,0:T(8,128)}, f32[40,256]{1,0:T(8,128)}, f32[32,4096]{1,0:T(8,128)}) custom-call(bf16[4,1024,256]{2,1,0:T(8,128)(2,1)} %values_hbm.1, bf16[4,1024,256]{2,1,0:T(8,128)(2,1)} %gates_hbm.1, bf16[4096,4096]{1,0:T(8,128)(2,1)} %bitcast.9, bf16[256,4096]{1,0:T(8,128)(2,1)} %weight_hbm.1, ...), custom_call_target="tpu_custom_call" | custom-call | tf_op jit(solution)/shard_map/fused/pallas_call | solution.py:517
  79.4 8.3 %finish.1 = (bf16[4096,256]{1,0:T(8,128)(2,1)}, bf16[4096,256]{1,0:T(8,128)(2,1)}, f32[31,256]{1,0:T(8,128)}, f32[1,256]{1,0:T(1,128)}, f32[1,256]{1,0:T(1,128)}, /*index=5*/f32[32,4096]{1,0:T(8,128)}) custom-call(f32[4096,256]{1,0:T(8,128)} %bitcast.12, f32[128,256]{1,0:T(8,128)} %bitcast.13, bf16[4096,256]{1,0:T(8,128)(2,1)} %bitcast.10, ...), custom_call_target="tpu_custom_call" | custom-call | tf_op jit(solution)/shard_map/finish/pallas_call | solution.py:593

commit v2 on v1

--- a/solution.py
+++ b/solution.py
@@ -86,14 +86,15 @@
 
 
 def fused_kernel(
-    total_chans, values_hbm, gates_hbm, cot_hbm, weight_hbm, table_hbm, taps_ref, bias_ref,
-    gain_ref,
-    spread_hbm, heads_ref, small_ref, weight_out_ref,
-    values, gates, values_halo, gates_halo, cot, swished, weight_t, weight_grad, pair, onward,
-    arrived, conv, grad, xpad, spectrum, high, low, grad_high, grad_low, table, tap_rows,
+    total_chans, values_hbm, gates_hbm, cot_hbm, weight_hbm, table_hbm, taps_hbm, bias_hbm,
+    gain_hbm,
+    spread_hbm, heads_hbm, small_hbm, weight_out_hbm,
+    values, gates, values_halo, gates_halo, cot, swished, weight, weight_t, weight_grad, pair,
+    onward, arrived, weight_sum, conv, grad, x_first, x_last, spectrum, high, low, grad_high, grad_low, table,
+    taps, bias_row, gain_row, tap_rows,
     tap_re, tap_im, corr_re, corr_im, heads, heads_in, sums, sums_in, stat, back, back_in,
-    gain_acc, bias_acc, small, small_in,
-    load_sems, cot_sems, misc_sems, out_sems, halo_send, halo_recv, sums_send, sums_recv,
+    gain_acc, bias_acc, small, small_sum, small_in,
+    load_sems, cot_sems, misc_sems, out_sems, weight_sems, halo_send, halo_recv, sums_send, sums_recv,
     back_send, back_recv, pair_send, pair_recv, onward_send, onward_recv, head_send, head_recv,
     small_send, small_recv,
 ):
@@ -102,7 +103,10 @@
     lane_blocks = chans // LANES
     chunks = tokens // LANES
     windows = spectrum.shape[0] // seqs
-    blocks, rows = cot_sems.shape[0], grad.shape[1]
+    rows = grad.shape[1]
+    blocks = positions // rows
+    strips = cot_sems.shape[0]
+    strip_width = width // strips
     seq_blocks = blocks // seqs
     block_chunks = rows // LANES
     parts = pair_send.shape[0]
@@ -115,28 +119,36 @@
     tp_peers = range(1, lax.axis_size("tp"))
     sp_peers = range(1, sp_devices)
 
-    loads = []
-    for n, (src, dst) in enumerate(((weight_hbm, swished.at[:, :width]), (table_hbm, table))):
-        copy = pltpu.make_async_copy(src, dst, misc_sems.at[n])
-        copy.start()
-        loads.append(copy)
-
     def seq_loads(s):
         return [
             pltpu.make_async_copy(src.at[s], dst.at[s], load_sems.at[n, s])
             for n, (src, dst) in enumerate(((values_hbm, values), (gates_hbm, gates)))
         ]
 
-    for s in range(seqs):
+    table_load = pltpu.make_async_copy(table_hbm, table, misc_sems.at[0])
+    row_loads = [
+        pltpu.make_async_copy(src, dst, misc_sems.at[n])
+        for n, (src, dst) in enumerate(
+            ((taps_hbm, taps), (bias_hbm, bias_row), (gain_hbm, gain_row)), 2
+        )
+    ]
+    weight_load = pltpu.make_async_copy(weight_hbm, weight, misc_sems.at[1])
+
+    def strip(i):
+        return pl.ds(pl.multiple_of(i * strip_width, strip_width), strip_width)
+
+    def cot_load(i):
+        return pltpu.make_async_copy(cot_hbm.at[:, strip(i)], cot.at[:, strip(i)], cot_sems.at[i])
+
+    for copy in row_loads:
+        copy.start()
+    for copy in seq_loads(0):
+        copy.start()
+    table_load.start()
+    for s in range(1, seqs):
         for copy in seq_loads(s):
             copy.start()
-
-    def cot_load(i):
-        here = pl.ds(pl.multiple_of(i * rows, rows), rows)
-        return pltpu.make_async_copy(cot_hbm.at[here], cot.at[here], cot_sems.at[i])
-
-    for i in range(blocks):
-        cot_load(i).start()
+    weight_load.start()
 
     greet([("tp", d) for d in tp_peers] + [("sp", d) for d in sp_peers])
     last = pl.ds(tokens - HALO, HALO)
@@ -147,31 +159,50 @@
     for copy in halo_copies:
         copy.start()
 
-    xpad[HALO + tokens :, :] = jnp.zeros((xpad.shape[0] - HALO - tokens, chans), BF16)
+    tail = tokens - (windows - 1) * STEP + HALO
+    x_last[tail:, :] = jnp.zeros((SPAN - tail, chans), BF16)
     for ref in (grad_high, grad_low):
         ref[tokens:, :] = jnp.zeros((ref.shape[0] - tokens, chans), BF16)
     for ref in (gain_acc, bias_acc, corr_re, corr_im, tap_rows):
         ref[...] = jnp.zeros_like(ref)
-    tap_rows[:K, :] = taps_ref[...].astype(F32)
-    bias = bias_ref[...].astype(F32).reshape(1, chans)
-    gain = gain_ref[...].astype(F32).reshape(1, chans)
-
-    for copy in loads:
+    for copy in row_loads:
         copy.wait()
+    tap_rows[:K, :] = taps[...].astype(F32)
+    bias = bias_row[...].astype(F32).reshape(1, chans)
+    gain = gain_row[...].astype(F32).reshape(1, chans)
+
+    table_load.wait()
     taps_wide = dot(table[TAPF : TAPF + 2 * SPAN], tap_rows[...].astype(BF16))
     taps_wide = taps_wide[:SPAN] + taps_wide[SPAN:]
     for q in range(SPAN // 16):
         tap_re[8 * q : 8 * q + 8, :] = taps_wide[16 * q : 16 * q + 8]
         tap_im[8 * q : 8 * q + 8, :] = taps_wide[16 * q + 8 : 16 * q + 16]
 
+    def gate(values_part, gates_part):
+        return (values_part.astype(F32) * sigmoid(gates_part.astype(F32))).astype(BF16)
+
+    def gate_all(s, carry):
+        for copy in seq_loads(s):
+            copy.wait()
+        for i in range(chunks):
+            here = slice(i * LANES, (i + 1) * LANES)
+            gated = gate(values[s, here, :], gates[s, here, :])
+            values[s, here, :] = gated
+            count = min(STEP - i * LANES, LANES)
+            if count > 0:
+                x_first[s, HALO + i * LANES : HALO + i * LANES + count, :] = gated[:count]
+        return carry
+
+    lax.fori_loop(0, seqs, gate_all, 0)
+    for i in range(strips):
+        cot_load(i).start()
+
     def turn(i, carry):
         here = pl.ds(pl.multiple_of(i * 512, 512), 512)
-        weight_t[here, :] = swished[:, here].T
+        weight_t[here, :] = weight[:, here].T
         return carry
 
-    lax.fori_loop(0, width // 512, turn, 0)
-
-    def product(x, w, sign):
+    def product(x, sign, high_ref, low_ref):
         for q in range(SPAN // 16):
             a, b = tap_re[8 * q : 8 * q + 8, :], tap_im[8 * q : 8 * q + 8, :]
             re, im = x[16 * q : 16 * q + 8], x[16 * q + 8 : 16 * q + 16]
@@ -180,7 +211,7 @@
             else:
                 both = (a * re + b * im, a * im - b * re)
             here = slice(16 * q, 16 * q + 16)
-            high[w, here, :], low[w, here, :] = split(jnp.concatenate(both, axis=0))
+            high_ref[here, :], low_ref[here, :] = split(jnp.concatenate(both, axis=0))
 
     def sums_copies(s):
         return [
@@ -189,27 +220,27 @@
             for d in tp_peers
         ]
 
+    weight_load.wait()
+    lax.fori_loop(0, width // 512, turn, 0)
     for copy in halo_copies:
         copy.wait()
     keep = jnp.where(me > 0, 1.0, 0.0).astype(F32)
-
-    def gate(values_part, gates_part):
-        return values_part.astype(F32) * sigmoid(gates_part.astype(F32))
+    for s in range(seqs):
+        x_first[s, :HALO, :] = gate(values_halo[s].astype(F32) * keep, gates_halo[s])
 
     def ahead(s, carry):
-        for copy in seq_loads(s):
-            copy.wait()
-        xpad[:HALO, :] = (gate(values_halo[s], gates_halo[s]) * keep).astype(BF16)
-        for i in range(chunks):
-            here = slice(i * LANES, (i + 1) * LANES)
-            xpad[HALO + i * LANES : HALO + (i + 1) * LANES, :] = gate(
-                values[s, here, :], gates[s, here, :]
-            ).astype(BF16)
+        x_last[:tail, :] = values[s, tokens - tail :, :]
         for w in range(windows):
-            x = dot(table[FWD : FWD + 2 * SPAN], xpad[w * STEP : w * STEP + SPAN, :])
+            if w == 0:
+                x = x_first[s]
+            elif w < windows - 1:
+                x = values[s, w * STEP - HALO : w * STEP + STEP, :]
+            else:
+                x = x_last[...]
+            x = dot(table[FWD : FWD + 2 * SPAN], x)
             x = x[:SPAN] + x[SPAN:]
             spectrum[s * windows + w] = x.astype(BF16)
-            product(x, w, 1)
+            product(x, 1, high.at[w], low.at[w])
         for w in range(windows):
             y = dot(table[CONV : CONV + 2 * STEP], high[w])
             y = y[:STEP] + y[STEP:] + dot(table[CONV : CONV + STEP], low[w]) + bias
@@ -248,13 +279,10 @@
                 normed = (conv[s, here, lanes] - mean) * inverse
                 conv[s, here, lanes] = normed
                 scaled = normed * gain[:, lanes]
-                swished[lanes, columns] = (scaled * sigmoid(scaled)).T.astype(BF16)
+                swished[lanes, columns] = (scaled * sigmoid(scaled)).astype(BF16).T
         return carry
 
     lax.fori_loop(0, seqs, norm, 0)
-
-    for i in range(blocks):
-        cot_load(i).wait()
 
     def part_columns(c):
         return pl.ds(pl.multiple_of(c * part_width, part_width), part_width)
@@ -272,18 +300,6 @@
             onward.at[d - 1, :, columns], arrived.at[d - 1, :, columns], onward_send.at[d - 1, c],
             onward_recv.at[d - 1, c], "sp", d * PAIR,
         )
-
-    def project(c, carry):
-        columns = part_columns(c)
-        result = dot(swished[:, :positions], cot[:, columns])
-        for g in range(groups):
-            for n in range(PAIR):
-                first = (g * PAIR + n) * weight_rows
-                weight_grad[n, g, :, columns] = result[first : first + weight_rows].astype(BF16)
-        pair_copy(c).start()
-        return carry
-
-    lax.fori_loop(0, parts, project, 0)
 
     def pass_on(c):
         columns = part_columns(c)
@@ -296,6 +312,27 @@
             ).astype(BF16)
         for d in range(1, groups):
             onward_copy(d, c).start()
+
+    def project(i, carry):
+        cot_load(i).wait()
+        result = dot(swished[...], cot[:, strip(i)])
+        for g in range(groups):
+            for n in range(PAIR):
+                first = (g * PAIR + n) * weight_rows
+                weight_grad[n, g, :, strip(i)] = result[first : first + weight_rows].astype(BF16)
+        for n in range(strip_parts):
+            pair_copy(i * strip_parts + n).start()
+
+        @pl.when(i >= lag)
+        def _():
+            pass_on(i - lag)
+
+        return carry
+
+    lag = min(3, strips)
+    strip_parts = parts // strips
+    lax.fori_loop(0, strips, project, 0)
+    passed = strips - lag
 
     def back_copies(j):
         return [
@@ -342,15 +379,18 @@
         middle(j - 1)
         multiply(j)
 
-        @pl.when(lax.rem(j, 2) == 0)
+        @pl.when(passed + j - 1 < parts)
         def _():
-            pass_on(j // 2 - 1)
+            pass_on(passed + j - 1)
 
         return carry
 
     lax.fori_loop(1, blocks, both, 0)
     middle(blocks - 1)
-    passed = min((blocks - 1) // 2, parts)
+    passed_on = passed + blocks - 1
+    if passed_on < parts:
+        pass_on(passed_on)
+        passed_on += 1
 
     def spread_copy(s):
         return pltpu.make_async_copy(conv.at[s], spread_hbm.at[s], out_sems.at[s])
@@ -359,6 +399,12 @@
         return remote(
             heads.at[s], heads_in.at[s], head_send.at[s], head_recv.at[s], "sp", sp_devices - 1
         )
+
+    per = tokens // SPAN
+
+    def spread_parts(s, w):
+        here = pl.ds(pl.multiple_of(s * tokens + w % per * SPAN, SPAN), SPAN)
+        return spectrum.at[s * windows + w], cot.at[here, pl.ds(w // per * chans, chans)]
 
     def behind(s, carry):
         for n in range(seq_blocks):
@@ -396,22 +442,11 @@
                 x_re, x_im = x[16 * q : 16 * q + 8], x[16 * q + 8 : 16 * q + 16]
                 corr_re[at, :] += g_re * x_re + g_im * x_im
                 corr_im[at, :] += g_im * x_re - g_re * x_im
-            product(g, w, -1)
-        for w in range(windows):
-            y = dot(table[INV : INV + 2 * SPAN], high[w])
-            y = y[:SPAN] + y[SPAN:] + dot(table[INV : INV + SPAN], low[w])
-            if w == 0:
-                heads[s] = y[:HALO]
-            else:
-                conv[s, w * STEP - HALO : w * STEP, :] += y[:HALO]
-            count = min(STEP, tokens - w * STEP)
-            conv[s, w * STEP : w * STEP + count, :] = y[HALO : HALO + count]
-        spread_copy(s).start()
-        head_copy(s).start()
-
-        @pl.when(passed + s < parts)
+            product(g, -1, *spread_parts(s, w))
+
+        @pl.when(passed_on + s < parts)
         def _():
-            pass_on(passed + s)
+            pass_on(passed_on + s)
 
         return carry
 
@@ -427,25 +462,44 @@
     small[32:33, :] = jnp.sum(bias_acc[...], axis=0, keepdims=True)
     small[33:34, :] = jnp.sum(gain_acc[...], axis=0, keepdims=True)
     small[34:, :] = jnp.zeros((small.shape[0] - 34, chans), F32)
+    small_pair = remote(
+        small, small_in.at[0], small_send.at[0], small_recv.at[0], "sp",
+        sp_devices + 1 - 2 * inner,
+    )
+    small_pair.start()
+    for c in range(min(passed_on + seqs, parts), parts):
+        pass_on(c)
+
+    def spread_window(s, w):
+        high_ref, low_ref = spread_parts(s, w)
+        y = dot(table[INV : INV + 2 * SPAN], high_ref[...])
+        y = y[:SPAN] + y[SPAN:] + dot(table[INV : INV + SPAN], low_ref[...])
+        count = min(STEP, tokens - w * STEP)
+        conv[s, w * STEP : w * STEP + count, :] = y[HALO : HALO + count]
+        return y[:HALO]
+
+    for s in range(seqs):
+        heads[s] = spread_window(s, 0)
+    for s in range(seqs):
+        head_copy(s).start()
+    small_pair.wait()
+    small_sum[...] = small[...] + small_in[0]
     small_copies = [
-        remote(small, small_in.at[d - 1], small_send.at[d - 1], small_recv.at[d - 1], "sp", d)
-        for d in sp_peers
+        remote(small_sum, small_in.at[d], small_send.at[d], small_recv.at[d], "sp", d * PAIR)
+        for d in range(1, groups)
     ]
     for copy in small_copies:
         copy.start()
 
-    for c in range(min(passed + seqs, parts), parts):
-        pass_on(c)
-
-    keep_head = jnp.where(me < sp_devices - 1, 1.0, 0.0).astype(F32)
-    for s in range(seqs):
-        head_copy(s).wait()
-        heads_ref[s] = heads_in[s] * keep_head
-    total = small[...]
-    for d, copy in zip(sp_peers, small_copies):
-        copy.wait()
-        total = total + small_in[d - 1]
-    small_ref[...] = total
+    def spread_rest(s, carry):
+        for w in range(1, windows):
+            conv[s, w * STEP - HALO : w * STEP, :] += spread_window(s, w)
+        spread_copy(s).start()
+        return carry
+
+    lax.fori_loop(0, seqs, spread_rest, 0)
+
+    outs = []
     for c in range(parts):
         columns = slice(c * part_width, (c + 1) * part_width)
         result = weight_grad[inner, outer, :, columns].astype(F32)
@@ -453,40 +507,98 @@
         for d in range(1, groups):
             onward_copy(d, c).wait()
             result = result + arrived[d - 1, :, columns].astype(F32)
-        weight_out_ref[:, columns] = result
+        weight_sum[:, columns] = result
+        if (c + 1) % strip_parts == 0:
+            columns = pl.ds(c // strip_parts * strip_width, strip_width)
+            outs.append(pltpu.make_async_copy(
+                weight_sum.at[:, columns], weight_out_hbm.at[:, columns],
+                weight_sems.at[c // strip_parts],
+            ))
+            outs[-1].start()
+    keep_head = jnp.where(me < sp_devices - 1, 1.0, 0.0).astype(F32)
+    for s in range(seqs):
+        head_copy(s).wait()
+        heads_in[s] = heads_in[s] * keep_head
+    outs.append(pltpu.make_async_copy(heads_in, heads_hbm, misc_sems.at[0]))
+    outs[-1].start()
+    total = small_sum[...]
+    for d, copy in enumerate(small_copies, 1):
+        copy.wait()
+        total = total + small_in[d]
+    small[...] = total
+    outs.append(pltpu.make_async_copy(small, small_hbm, misc_sems.at[1]))
+    outs[-1].start()
+    for copy in outs:
+        copy.wait()
     for s in range(seqs):
         spread_copy(s).wait()
 
 
 def finish_kernel(
-    seq_blocks, spread_ref, heads_ref, values_ref, gates_ref, small_ref, weight_ref,
-    values_grad_ref, gates_grad_ref, taps_grad_ref, gain_grad_ref, bias_grad_ref, weight_grad_ref,
-    gated_grad,
+    spread_hbm, values_hbm, gates_hbm, weight_hbm, heads_hbm, small_hbm,
+    values_grad_hbm, gates_grad_hbm, weight_grad_hbm, taps_grad_hbm, gain_grad_hbm, bias_grad_hbm,
+    spread, values, gates, weight, heads, small, taps_grad, gain_grad, bias_grad,
+    load_sems, out_sems, in_sems, end_sems,
 ):
-    step = pl.program_id(0)
-    rows = spread_ref.shape[0]
-    share = jnp.where(lax.rem(step, seq_blocks) == seq_blocks - 1, 1.0, 0.0).astype(F32)
-
-    @pl.when(step == 0)
-    def _():
-        taps_grad_ref[...] = small_ref[:K]
-        bias_grad_ref[...] = small_ref[32:33]
-        gain_grad_ref[...] = small_ref[33:34]
-        weight_grad_ref[...] = weight_ref[...]
-
-    gated_grad[...] = spread_ref[...]
-    gated_grad[rows - HALO :, :] += heads_ref[...] * share
-    for i in range(rows // LANES):
-        here = slice(i * LANES, (i + 1) * LANES)
-        sig = sigmoid(gates_ref[here, :].astype(F32))
-        values_part = gated_grad[here, :] * sig
-        values_grad_ref[here, :] = values_part.astype(BF16)
-        gates_part = values_part * values_ref[here, :].astype(F32) * (1.0 - sig)
-        gates_grad_ref[here, :] = gates_part.astype(BF16)
-
-
-def whole(shape):
-    return pl.BlockSpec(shape, lambda i: (0,) * len(shape))
+    seqs, tokens, chans = spread.shape
+    seq_blocks = load_sems.shape[1] // seqs
+    rows = tokens // seq_blocks
+    loads, stores = [], []
+    extra = [
+        pltpu.make_async_copy(src, dst, in_sems.at[n])
+        for n, (src, dst) in enumerate(
+            ((heads_hbm, heads), (small_hbm, small), (weight_hbm, weight))
+        )
+    ]
+    ends = [
+        pltpu.make_async_copy(src, dst, end_sems.at[n])
+        for n, (src, dst) in enumerate((
+            (taps_grad, taps_grad_hbm), (gain_grad, gain_grad_hbm), (bias_grad, bias_grad_hbm),
+            (weight, weight_grad_hbm),
+        ))
+    ]
+    for copy in extra[:2]:
+        copy.start()
+    for n in range(seqs * seq_blocks):
+        s, here = n // seq_blocks, pl.ds(n % seq_blocks * rows, rows)
+        pairs = ((spread_hbm, spread), (values_hbm, values), (gates_hbm, gates))
+        loads.append([
+            pltpu.make_async_copy(src.at[s, here], dst.at[s, here], load_sems.at[m, n])
+            for m, (src, dst) in enumerate(pairs)
+        ])
+        for copy in loads[n]:
+            copy.start()
+    extra[2].start()
+    for copy in extra[:2]:
+        copy.wait()
+    taps_grad[...] = small[:K]
+    bias_grad[...] = small[32:33]
+    gain_grad[...] = small[33:34]
+    for copy in ends[:3]:
+        copy.start()
+    for n in range(seqs * seq_blocks):
+        s, first = n // seq_blocks, n % seq_blocks * rows
+        for copy in loads[n]:
+            copy.wait()
+        if n % seq_blocks == seq_blocks - 1:
+            spread[s, tokens - HALO :, :] += heads[s]
+        for i in range(rows // LANES):
+            here = slice(first + i * LANES, first + (i + 1) * LANES)
+            sig = sigmoid(gates[s, here, :].astype(F32))
+            values_part = spread[s, here, :] * sig
+            gates_part = values_part * values[s, here, :].astype(F32) * (1.0 - sig)
+            values[s, here, :] = values_part.astype(BF16)
+            gates[s, here, :] = gates_part.astype(BF16)
+        for m, (src, dst) in enumerate(((values, values_grad_hbm), (gates, gates_grad_hbm))):
+            copy = pltpu.make_async_copy(
+                src.at[s, pl.ds(first, rows)], dst.at[s, pl.ds(first, rows)], out_sems.at[m, n]
+            )
+            copy.start()
+            stores.append(copy)
+    extra[2].wait()
+    ends[3].start()
+    for copy in stores + ends:
+        copy.wait()
 
 
 def on_device(values_in, gates_in, conv_taps, conv_bias, norm_gain, out_weight, out_grad):
@@ -496,13 +608,12 @@
     positions = seqs * tokens
     rows = min(512, tokens)
     blocks = positions // rows
-    seq_blocks = tokens // rows
     chunks = tokens // LANES
     windows = -(-tokens // STEP)
-    parts = 8
+    strips = 8
+    parts = 16
     tp_others = lax.axis_size("tp") - 1
     sp_devices = lax.axis_size("sp")
-    sp_others = sp_devices - 1
     groups = sp_devices // PAIR
     weight_rows = chans // sp_devices
     small_rows = 40
@@ -511,13 +622,12 @@
         return pltpu.SemaphoreType.DMA(shape)
 
     anywhere = pl.BlockSpec(memory_space=pl.ANY)
-    vmem = pl.BlockSpec(memory_space=pltpu.VMEM)
     padded = windows * STEP + HALO
     block_sums = (2, rows // LANES, LANES)
     spread, heads, small, weight_sum = pl.pallas_call(
         functools.partial(fused_kernel, total_chans),
-        in_specs=[anywhere] * 5 + [vmem] * 3,
-        out_specs=[anywhere] + [vmem] * 3,
+        in_specs=[anywhere] * 8,
+        out_specs=[anywhere] * 4,
         out_shape=[
             jax.ShapeDtypeStruct((seqs, tokens, chans), F32),
             jax.ShapeDtypeStruct((seqs, HALO, chans), F32),
@@ -530,21 +640,27 @@
             pltpu.VMEM((seqs, HALO, chans), BF16),
             pltpu.VMEM((seqs, HALO, chans), BF16),
             pltpu.VMEM((positions, width), BF16),
-            pltpu.VMEM((chans, max(positions, width)), BF16),
+            pltpu.VMEM((chans, positions), BF16),
+            pltpu.VMEM((chans, width), BF16),
             pltpu.VMEM((width, chans), BF16),
             pltpu.VMEM((PAIR, groups, weight_rows, width), BF16),
             pltpu.VMEM((groups, weight_rows, width), BF16),
             pltpu.VMEM((groups - 1, weight_rows, width), BF16),
             pltpu.VMEM((groups - 1, weight_rows, width), BF16),
+            pltpu.VMEM((weight_rows, width), F32),
             pltpu.VMEM((seqs, tokens, chans), F32),
             pltpu.VMEM((2, rows, chans), F32),
-            pltpu.VMEM((padded, chans), BF16),
+            pltpu.VMEM((seqs, SPAN, chans), BF16),
+            pltpu.VMEM((SPAN, chans), BF16),
             pltpu.VMEM((seqs * windows, SPAN, chans), BF16),
             pltpu.VMEM((windows, SPAN, chans), BF16),
             pltpu.VMEM((windows, SPAN, chans), BF16),
             pltpu.VMEM((padded, chans), BF16),
             pltpu.VMEM((padded, chans), BF16),
             pltpu.VMEM((TABLE_ROWS, SPAN), BF16),
+            pltpu.VMEM((K, chans), BF16),
+            pltpu.VMEM((chans,), BF16),
+            pltpu.VMEM((chans,), BF16),
             pltpu.VMEM((SPAN, chans), F32),
             pltpu.VMEM((SPAN // 2, chans), F32),
             pltpu.VMEM((SPAN // 2, chans), F32),
@@ -560,11 +676,13 @@
             pltpu.VMEM((8, chans), F32),
             pltpu.VMEM((8, chans), F32),
             pltpu.VMEM((small_rows, chans), F32),
-            pltpu.VMEM((sp_others, small_rows, chans), F32),
+            pltpu.VMEM((small_rows, chans), F32),
+            pltpu.VMEM((groups, small_rows, chans), F32),
             dma(2, seqs),
-            dma(blocks),
-            dma(2),
+            dma(strips),
+            dma(5),
             dma(seqs),
+            dma(strips),
             dma(2),
             dma(2),
             dma(tp_others, seqs),
@@ -577,8 +695,8 @@
             dma(groups - 1, parts),
             dma(seqs),
             dma(seqs),
-            dma(sp_others),
-            dma(sp_others),
+            dma(groups),
+            dma(groups),
         ],
         compiler_params=pltpu.CompilerParams(
             vmem_limit_bytes=VMEM_LIMIT, collective_id=0, has_side_effects=True
@@ -589,42 +707,37 @@
         jnp.asarray(transform_table()), conv_taps, conv_bias, norm_gain,
     )
 
-    tile = pl.BlockSpec((rows, chans), lambda i: (i, 0))
-    values_grad, gates_grad, taps_grad, gain_grad, bias_grad, weight_grad = pl.pallas_call(
-        functools.partial(finish_kernel, seq_blocks),
-        grid=(blocks,),
-        in_specs=[
-            tile, pl.BlockSpec((HALO, chans), lambda i: (i // seq_blocks, 0)), tile, tile,
-            whole((small_rows, chans)), whole((weight_rows, width)),
-        ],
-        out_specs=[
-            tile, tile, whole((K, chans)), whole((1, chans)), whole((1, chans)),
-            whole((weight_rows, width)),
-        ],
+    values_grad, gates_grad, weight_grad, taps_grad, gain_grad, bias_grad = pl.pallas_call(
+        finish_kernel,
+        in_specs=[anywhere] * 6,
+        out_specs=[anywhere] * 6,
         out_shape=[
-            jax.ShapeDtypeStruct((positions, chans), BF16),
-            jax.ShapeDtypeStruct((positions, chans), BF16),
+            jax.ShapeDtypeStruct((seqs, tokens, chans), BF16),
+            jax.ShapeDtypeStruct((seqs, tokens, chans), BF16),
+            jax.ShapeDtypeStruct((weight_rows, width), F32),
             jax.ShapeDtypeStruct((K, chans), F32),
             jax.ShapeDtypeStruct((1, chans), F32),
             jax.ShapeDtypeStruct((1, chans), F32),
-            jax.ShapeDtypeStruct((weight_rows, width), F32),
         ],
-        scratch_shapes=[pltpu.VMEM((rows, chans), F32)],
-        compiler_params=pltpu.CompilerParams(dimension_semantics=("arbitrary",)),
+        scratch_shapes=[
+            pltpu.VMEM((seqs, tokens, chans), F32),
+            pltpu.VMEM((seqs, tokens, chans), BF16),
+            pltpu.VMEM((seqs, tokens, chans), BF16),
+            pltpu.VMEM((weight_rows, width), F32),
+            pltpu.VMEM((seqs, HALO, chans), F32),
+            pltpu.VMEM((small_rows, chans), F32),
+            pltpu.VMEM((K, chans), F32),
+            pltpu.VMEM((1, chans), F32),
+            pltpu.VMEM((1, chans), F32),
+            dma(3, blocks),
+            dma(2, blocks),
+            dma(3),
+            dma(4),
+        ],
+        compiler_params=pltpu.CompilerParams(vmem_limit_bytes=VMEM_LIMIT),
         name="finish",
-    )(
-        spread.reshape(positions, chans), heads.reshape(seqs * HALO, chans),
-        values_in.reshape(positions, chans), gates_in.reshape(positions, chans),
-        small, weight_sum,
-    )
-    return (
-        values_grad.reshape(values_in.shape),
-        gates_grad.reshape(values_in.shape),
-        taps_grad,
-        gain_grad[0],
-        bias_grad[0],
-        weight_grad,
-    )
+    )(spread, values_in, gates_in, weight_sum, heads, small)
+    return values_grad, gates_grad, taps_grad, gain_grad[0], bias_grad[0], weight_grad
 
 
 def solution(mesh):

time: 88.1 us -> 67 us (0.76)
  Pallas kernels: 87.1 us -> 66.2 us
    pallas_call x1, Pallas kernels: 78.8 us -> 60.1 us  [on_device(): pl.pallas_call(functools.partial(fused_kernel, total_chans), in_specs=[an...]
    pallas_call x1, Pallas kernels: 8.31 us -> 6.13 us  [on_device(): pl.pallas_call(finish_kernel, in_specs=[anywhere] * 6, out_specs=[anywher...]
where the time goes in v2:
time: 67 us; the launch traced here: 66.9 us
  Pallas kernels  66.2 us (99%)
    pallas_call x1, Pallas kernels, on_device(): pl.pallas_call(functools.partial(fused_kernel, total_chans), in_specs=[an...  60.1 us
    pallas_call x1, Pallas kernels, on_device(): pl.pallas_call(finish_kernel, in_specs=[anywhere] * 6, out_specs=[anywher...  6.13 us

profile of v2, /device:TPU:0, one launch (start us, length us, event | category | flops | bytes accessed | tf_op | source)
XLA Modules:
  0.0 66.9 jit_solution(5442091676561303108)
XLA Ops:
  0.6 60.1 %fused.1 = (f32[4,1024,256]{2,1,0:T(8,128)}, f32[4,32,256]{2,1,0:T(8,128)}, f32[40,256]{1,0:T(8,128)}, f32[32,4096]{1,0:T(8,128)}) custom-call(bf16[4,1024,256]{2,1,0:T(8,128)(2,1)} %values_hbm.3, bf16[4,1024,256]{2,1,0:T(8,128)(2,1)} %gates_hbm.3, bf16[4096,4096]{1,0:T(8,128)(2,1)} %bitcast.3, bf16[256,4096]{1,0:T(8,128)(2,1)} %weight_hbm.1, ...), custom_call_target="tpu_custom_call" | custom-call | tf_op jit(solution)/shard_map/fused/pallas_call | solution.py:627
  60.7 6.1 %finish.1 = (bf16[4,1024,256]{2,1,0:T(8,128)(2,1)}, bf16[4,1024,256]{2,1,0:T(8,128)(2,1)}, f32[32,4096]{1,0:T(8,128)}, f32[31,256]{1,0:T(8,128)}, f32[1,256]{1,0:T(1,128)}, /*index=5*/f32[1,256]{1,0:T(1,128)}) custom-call(f32[4,1024,256]{2,1,0:T(8,128)} %get-tuple-element.16.spread_hbm, bf16[4,1024,256]{2,1,0:T(8,128)(2,1)} %values_hbm.3, ...), custom_call_target="tpu_custom_call" | custom-call | tf_op jit(solution)/shard_map/finish/pallas_call | solution.py:710

commit v3 on v2

--- a/solution.py
+++ b/solution.py
@@ -68,6 +68,10 @@
     )
 
 
+def arrive(ref, sem, axis):
+    remote(ref, ref, sem, sem, axis, 1).wait_recv()
+
+
 def dot(a, b):
     return jnp.dot(a, b, preferred_element_type=F32)
 
@@ -88,13 +92,13 @@
 def fused_kernel(
     total_chans, values_hbm, gates_hbm, cot_hbm, weight_hbm, table_hbm, taps_hbm, bias_hbm,
     gain_hbm,
-    spread_hbm, heads_hbm, small_hbm, weight_out_hbm,
-    values, gates, values_halo, gates_halo, cot, swished, weight, weight_t, weight_grad, pair,
-    onward, arrived, weight_sum, conv, grad, x_first, x_last, spectrum, high, low, grad_high, grad_low, table,
+    values_grad_hbm, gates_grad_hbm, small_hbm, weight_out_hbm,
+    values, gates, values_halo, gates_halo, cot, swished, weight_t, weight_grad, pair,
+    onward, arrived, weight_sum, conv, norm_grad, grad, x_first, x_last, spectrum, high, low, grad_high, grad_low, table,
     taps, bias_row, gain_row, tap_rows,
     tap_re, tap_im, corr_re, corr_im, heads, heads_in, sums, sums_in, stat, back, back_in,
-    gain_acc, bias_acc, small, small_sum, small_in,
-    load_sems, cot_sems, misc_sems, out_sems, weight_sems, halo_send, halo_recv, sums_send, sums_recv,
+    gain_acc, bias_acc, small, small_sum, small_total, small_in,
+    load_sems, cot_sems, misc_sems, halo_send, halo_recv, sums_send, sums_recv,
     back_send, back_recv, pair_send, pair_recv, onward_send, onward_recv, head_send, head_recv,
     small_send, small_recv,
 ):
@@ -109,7 +113,7 @@
     strip_width = width // strips
     seq_blocks = blocks // seqs
     block_chunks = rows // LANES
-    parts = pair_send.shape[0]
+    parts = pair_recv.shape[0]
     part_width = width // parts
     groups, weight_rows = pair.shape[0], pair.shape[1]
     sp_devices = lax.axis_size("sp")
@@ -132,7 +136,9 @@
             ((taps_hbm, taps), (bias_hbm, bias_row), (gain_hbm, gain_row)), 2
         )
     ]
-    weight_load = pltpu.make_async_copy(weight_hbm, weight, misc_sems.at[1])
+    weight_load = pltpu.make_async_copy(
+        weight_hbm, swished.at[:, :width], misc_sems.at[1]
+    )
 
     def strip(i):
         return pl.ds(pl.multiple_of(i * strip_width, strip_width), strip_width)
@@ -199,7 +205,7 @@
 
     def turn(i, carry):
         here = pl.ds(pl.multiple_of(i * 512, 512), 512)
-        weight_t[here, :] = weight[:, here].T
+        weight_t[here, :] = swished[:, here].T
         return carry
 
     def product(x, sign, high_ref, low_ref):
@@ -215,8 +221,7 @@
 
     def sums_copies(s):
         return [
-            remote(sums.at[s], sums_in.at[d - 1, s], sums_send.at[d - 1, s],
-                   sums_recv.at[d - 1, s], "tp", d)
+            remote(sums.at[s], sums_in.at[d - 1, s], sums_send, sums_recv.at[s], "tp", d)
             for d in tp_peers
         ]
 
@@ -259,30 +264,43 @@
         return carry
 
     lax.fori_loop(0, seqs, ahead, 0)
-
-    def norm(s, carry):
-        total = sums[s]
-        for d, copy in zip(tp_peers, sums_copies(s)):
-            copy.wait()
-            total = total + sums_in[d - 1, s]
-        mean_rows = total[0] / total_chans
-        variance = total[1] / total_chans - mean_rows * mean_rows
-        inverse_rows = lax.rsqrt(variance + EPS)
-        stat[s] = inverse_rows
-        for i in range(chunks):
-            here = slice(i * LANES, (i + 1) * LANES)
-            columns = pl.ds(pl.multiple_of(s * tokens + i * LANES, LANES), LANES)
-            mean = row_spread(mean_rows[i : i + 1])
-            inverse = row_spread(inverse_rows[i : i + 1])
-            for h in range(lane_blocks):
-                lanes = slice(h * LANES, (h + 1) * LANES)
-                normed = (conv[s, here, lanes] - mean) * inverse
-                conv[s, here, lanes] = normed
-                scaled = normed * gain[:, lanes]
-                swished[lanes, columns] = (scaled * sigmoid(scaled)).astype(BF16).T
-        return carry
-
-    lax.fori_loop(0, seqs, norm, 0)
+    for s in range(seqs):
+        seq_loads(s)[0].start()
+
+    side = 2 if seqs % 2 == 0 else 1
+    half_gain = 0.5 * gain
+
+    def norm(p, carry):
+        for s in range(side):
+            arrive(sums_in.at[:, p * side + s], sums_recv.at[p * side + s], "tp")
+        for n in range(side):
+            s = p * side + n
+            total = sums[s]
+            for d in tp_peers:
+                total = total + sums_in[d - 1, s]
+            mean_rows = total[0] / total_chans
+            variance = total[1] / total_chans - mean_rows * mean_rows
+            inverse_rows = lax.rsqrt(variance + EPS)
+            stat[s] = inverse_rows
+            def spreads(i):
+                return row_spread(mean_rows[i : i + 1]), row_spread(inverse_rows[i : i + 1])
+
+            following = spreads(0)
+            for i in range(chunks):
+                here = slice(i * LANES, (i + 1) * LANES)
+                columns = pl.ds(pl.multiple_of(s * tokens + i * LANES, LANES), LANES)
+                mean, inverse = following
+                if i + 1 < chunks:
+                    following = spreads(i + 1)
+                for h in range(lane_blocks):
+                    lanes = slice(h * LANES, (h + 1) * LANES)
+                    normed = (conv[s, here, lanes] - mean) * inverse
+                    conv[s, here, lanes] = normed
+                    half = normed * half_gain[:, lanes]
+                    swished[lanes, columns] = (half * jnp.tanh(half) + half).astype(BF16).T
+        return carry
+
+    lax.fori_loop(0, seqs // side, norm, 0)
 
     def part_columns(c):
         return pl.ds(pl.multiple_of(c * part_width, part_width), part_width)
@@ -290,20 +308,20 @@
     def pair_copy(c):
         columns = part_columns(c)
         return remote(
-            weight_grad.at[1 - inner, :, :, columns], pair.at[:, :, columns], pair_send.at[c],
+            weight_grad.at[1 - inner, :, :, columns], pair.at[:, :, columns], pair_send,
             pair_recv.at[c], "sp", sp_devices + 1 - 2 * inner,
         )
 
     def onward_copy(d, c):
         columns = part_columns(c)
         return remote(
-            onward.at[d - 1, :, columns], arrived.at[d - 1, :, columns], onward_send.at[d - 1, c],
-            onward_recv.at[d - 1, c], "sp", d * PAIR,
+            onward.at[d - 1, :, columns], arrived.at[d - 1, :, columns], onward_send,
+            onward_recv, "sp", d * PAIR,
         )
 
     def pass_on(c):
         columns = part_columns(c)
-        pair_copy(c).wait()
+        pair_copy(c).wait_recv()
         for d in range(1, groups):
             target = lax.rem(outer + d, groups)
             onward[d - 1, :, columns] = (
@@ -315,7 +333,7 @@
 
     def project(i, carry):
         cot_load(i).wait()
-        result = dot(swished[...], cot[:, strip(i)])
+        result = dot(swished[:, :positions], cot[:, strip(i)])
         for g in range(groups):
             for n in range(PAIR):
                 first = (g * PAIR + n) * weight_rows
@@ -336,8 +354,8 @@
 
     def back_copies(j):
         return [
-            remote(back.at[j], back_in.at[d - 1, j], back_send.at[d - 1, j],
-                   back_recv.at[d - 1, j], "tp", d)
+            remote(back.at[j], back_in.at[d - 1, j], back_send, back_recv.at[j // seq_blocks],
+                   "tp", d)
             for d in tp_peers
         ]
 
@@ -345,7 +363,7 @@
         here = pl.ds(pl.multiple_of(j * rows, rows), rows)
         grad[lax.rem(j, 2)] = dot(cot[here, :], weight_t[...])
 
-    def middle(j):
+    def middle(j, following=None):
         s = j // seq_blocks
         first = lax.rem(j, seq_blocks) * rows
         slot = lax.rem(j, 2)
@@ -362,7 +380,7 @@
                     sig + silu * (1.0 - sig)
                 )
                 normed_grad = scaled_grad * gain[:, lanes]
-                values[s, here, lanes], gates[s, here, lanes] = split(normed_grad)
+                norm_grad[s, here, lanes] = normed_grad
                 term = scaled_grad * normed
                 gain_acc[:, lanes] += jnp.sum(term.reshape(LANES // 8, 8, LANES), axis=0)
                 term = normed_grad * normed
@@ -370,14 +388,20 @@
                 weighted = term if weighted is None else weighted + term
             back[j, 0, i : i + 1, :] = lane_sums(plain)
             back[j, 1, i : i + 1, :] = lane_sums(weighted)
+            if following is not None:
+                deep = slice(i * width // block_chunks, (i + 1) * width // block_chunks)
+                here = pl.ds(pl.multiple_of(following * rows, rows), rows)
+                part = dot(cot[here, deep], weight_t[deep, :])
+                result = part if i == 0 else result + part
+        if following is not None:
+            grad[lax.rem(following, 2)] = result
         for copy in back_copies(j):
             copy.start()
 
     multiply(0)
 
     def both(j, carry):
-        middle(j - 1)
-        multiply(j)
+        middle(j - 1, j)
 
         @pl.when(passed + j - 1 < parts)
         def _():
@@ -392,12 +416,15 @@
         pass_on(passed_on)
         passed_on += 1
 
-    def spread_copy(s):
-        return pltpu.make_async_copy(conv.at[s], spread_hbm.at[s], out_sems.at[s])
+    def grad_copies(s):
+        return [
+            pltpu.make_async_copy(src.at[s], dst.at[s], misc_sems.at[3 + n])
+            for n, (src, dst) in enumerate(((values, values_grad_hbm), (gates, gates_grad_hbm)))
+        ]
 
     def head_copy(s):
         return remote(
-            heads.at[s], heads_in.at[s], head_send.at[s], head_recv.at[s], "sp", sp_devices - 1
+            heads.at[s], heads_in.at[s], head_send, head_recv, "sp", sp_devices - 1
         )
 
     per = tokens // SPAN
@@ -406,10 +433,16 @@
         here = pl.ds(pl.multiple_of(s * tokens + w % per * SPAN, SPAN), SPAN)
         return spectrum.at[s * windows + w], cot.at[here, pl.ds(w // per * chans, chans)]
 
+    def spread_window(s, w):
+        high_ref, low_ref = spread_parts(s, w)
+        y = dot(table[INV : INV + 2 * SPAN], high_ref[...])
+        y = y[:SPAN] + y[SPAN:] + dot(table[INV : INV + SPAN], low_ref[...])
+        count = min(STEP, tokens - w * STEP)
+        conv[s, w * STEP : w * STEP + count, :] = y[HALO : HALO + count]
+        return y[:HALO]
+
     def behind(s, carry):
-        for n in range(seq_blocks):
-            for copy in back_copies(s * seq_blocks + n):
-                copy.wait()
+        arrive(back_in.at[:, pl.ds(s * seq_blocks, seq_blocks)], back_recv.at[s], "tp")
         for i in range(chunks):
             here = slice(i * LANES, (i + 1) * LANES)
             j = s * seq_blocks + i // block_chunks
@@ -425,10 +458,7 @@
             weighted = row_spread(weighted * scale)
             for h in range(lane_blocks):
                 lanes = slice(h * LANES, (h + 1) * LANES)
-                normed_grad = values[s, here, lanes].astype(F32) + gates[s, here, lanes].astype(
-                    F32
-                )
-                conv_grad = inverse * normed_grad - plain - conv[s, here, lanes] * weighted
+                conv_grad = inverse * norm_grad[s, here, lanes] - plain - conv[s, here, lanes] * weighted
                 grad_high[here, lanes], grad_low[here, lanes] = split(conv_grad)
                 bias_acc[:, lanes] += jnp.sum(conv_grad.reshape(LANES // 8, 8, LANES), axis=0)
         for w in range(windows):
@@ -443,6 +473,9 @@
                 corr_re[at, :] += g_re * x_re + g_im * x_im
                 corr_im[at, :] += g_im * x_re - g_re * x_im
             product(g, -1, *spread_parts(s, w))
+            if w == 0:
+                heads[s] = spread_window(s, 0).astype(BF16)
+        head_copy(s).start()
 
         @pl.when(passed_on + s < parts)
         def _():
@@ -463,141 +496,113 @@
     small[33:34, :] = jnp.sum(gain_acc[...], axis=0, keepdims=True)
     small[34:, :] = jnp.zeros((small.shape[0] - 34, chans), F32)
     small_pair = remote(
-        small, small_in.at[0], small_send.at[0], small_recv.at[0], "sp",
+        small, small_in.at[0], pair_send, small_recv.at[0], "sp",
         sp_devices + 1 - 2 * inner,
     )
     small_pair.start()
     for c in range(min(passed_on + seqs, parts), parts):
         pass_on(c)
 
-    def spread_window(s, w):
-        high_ref, low_ref = spread_parts(s, w)
-        y = dot(table[INV : INV + 2 * SPAN], high_ref[...])
-        y = y[:SPAN] + y[SPAN:] + dot(table[INV : INV + SPAN], low_ref[...])
-        count = min(STEP, tokens - w * STEP)
-        conv[s, w * STEP : w * STEP + count, :] = y[HALO : HALO + count]
-        return y[:HALO]
-
-    for s in range(seqs):
-        heads[s] = spread_window(s, 0)
-    for s in range(seqs):
-        head_copy(s).start()
-    small_pair.wait()
+    def spread_rest(s, carry):
+        for w in range(1, windows):
+            conv[s, w * STEP - HALO : w * STEP, :] += spread_window(s, w)
+        return carry
+
+    lax.fori_loop(0, seqs, spread_rest, 0)
+    small_pair.wait_recv()
     small_sum[...] = small[...] + small_in[0]
     small_copies = [
-        remote(small_sum, small_in.at[d], small_send.at[d], small_recv.at[d], "sp", d * PAIR)
+        remote(small_sum, small_in.at[d], small_send, small_recv.at[1], "sp", d * PAIR)
         for d in range(1, groups)
     ]
     for copy in small_copies:
         copy.start()
-
-    def spread_rest(s, carry):
-        for w in range(1, windows):
-            conv[s, w * STEP - HALO : w * STEP, :] += spread_window(s, w)
-        spread_copy(s).start()
-        return carry
-
-    lax.fori_loop(0, seqs, spread_rest, 0)
-
-    outs = []
+    keep_head = jnp.where(me < sp_devices - 1, 1.0, 0.0).astype(F32)
+    arrive(heads_in, head_recv, "sp")
+    for s in range(seqs):
+        seq_loads(s)[0].wait()
+
+    def finish(s, carry):
+        conv[s, tokens - HALO :, :] += heads_in[s].astype(F32) * keep_head
+        for i in range(chunks):
+            here = slice(i * LANES, (i + 1) * LANES)
+            sig = sigmoid(gates[s, here, :].astype(F32))
+            values_part = conv[s, here, :] * sig
+            gates_part = values_part * values[s, here, :].astype(F32) * (1.0 - sig)
+            values[s, here, :] = values_part.astype(BF16)
+            gates[s, here, :] = gates_part.astype(BF16)
+        for copy in grad_copies(s):
+            copy.start()
+        return carry
+
+    lax.fori_loop(0, seqs, finish, 0)
+
+    arrive(arrived, onward_recv, "sp")
     for c in range(parts):
         columns = slice(c * part_width, (c + 1) * part_width)
         result = weight_grad[inner, outer, :, columns].astype(F32)
         result = result + pair[outer, :, columns].astype(F32)
         for d in range(1, groups):
-            onward_copy(d, c).wait()
             result = result + arrived[d - 1, :, columns].astype(F32)
         weight_sum[:, columns] = result
         if (c + 1) % strip_parts == 0:
             columns = pl.ds(c // strip_parts * strip_width, strip_width)
-            outs.append(pltpu.make_async_copy(
-                weight_sum.at[:, columns], weight_out_hbm.at[:, columns],
-                weight_sems.at[c // strip_parts],
-            ))
-            outs[-1].start()
-    keep_head = jnp.where(me < sp_devices - 1, 1.0, 0.0).astype(F32)
-    for s in range(seqs):
-        head_copy(s).wait()
-        heads_in[s] = heads_in[s] * keep_head
-    outs.append(pltpu.make_async_copy(heads_in, heads_hbm, misc_sems.at[0]))
-    outs[-1].start()
+            pltpu.make_async_copy(
+                weight_sum.at[:, columns], weight_out_hbm.at[:, columns], misc_sems.at[2]
+            ).start()
+    arrive(small_in.at[1:], small_recv.at[1], "sp")
     total = small_sum[...]
-    for d, copy in enumerate(small_copies, 1):
-        copy.wait()
+    for d in range(1, groups):
         total = total + small_in[d]
-    small[...] = total
-    outs.append(pltpu.make_async_copy(small, small_hbm, misc_sems.at[1]))
-    outs[-1].start()
+    small_total[...] = total
+    outs = [pltpu.make_async_copy(small_total, small_hbm, misc_sems.at[1])]
+    outs[0].start()
+    for ref, sem, axis in (
+        (sums_in, sums_send, "tp"), (back_in, back_send, "tp"), (onward, onward_send, "sp"),
+        (pair, pair_send, "sp"), (small, pair_send, "sp"), (heads, head_send, "sp"),
+        (small_in.at[1:], small_send, "sp"),
+    ):
+        remote(ref, ref, sem, sem, axis, 1).wait_send()
+    outs.append(pltpu.make_async_copy(weight_sum, weight_out_hbm, misc_sems.at[2]))
+    outs.append(pltpu.make_async_copy(values, values_grad_hbm, misc_sems.at[3]))
+    outs.append(pltpu.make_async_copy(gates, gates_grad_hbm, misc_sems.at[4]))
     for copy in outs:
         copy.wait()
+
+
+def hand_over_kernel(
+    values_hbm, gates_hbm, weight_hbm, small_hbm,
+    values_grad_hbm, gates_grad_hbm, weight_grad_hbm, taps_grad_hbm, gain_grad_hbm, bias_grad_hbm,
+    values, gates, weight, small, taps_grad, gain_grad, bias_grad, in_sems, out_sems,
+):
+    seqs = values.shape[0]
+    pairs = [(small_hbm, small, None)]
     for s in range(seqs):
-        spread_copy(s).wait()
-
-
-def finish_kernel(
-    spread_hbm, values_hbm, gates_hbm, weight_hbm, heads_hbm, small_hbm,
-    values_grad_hbm, gates_grad_hbm, weight_grad_hbm, taps_grad_hbm, gain_grad_hbm, bias_grad_hbm,
-    spread, values, gates, weight, heads, small, taps_grad, gain_grad, bias_grad,
-    load_sems, out_sems, in_sems, end_sems,
-):
-    seqs, tokens, chans = spread.shape
-    seq_blocks = load_sems.shape[1] // seqs
-    rows = tokens // seq_blocks
-    loads, stores = [], []
-    extra = [
-        pltpu.make_async_copy(src, dst, in_sems.at[n])
-        for n, (src, dst) in enumerate(
-            ((heads_hbm, heads), (small_hbm, small), (weight_hbm, weight))
-        )
+        pairs.append((values_hbm.at[s], values.at[s], values_grad_hbm.at[s]))
+        pairs.append((gates_hbm.at[s], gates.at[s], gates_grad_hbm.at[s]))
+    pairs.append((weight_hbm, weight, weight_grad_hbm))
+    loads = [
+        pltpu.make_async_copy(src, here, in_sems.at[n]) for n, (src, here, _) in enumerate(pairs)
     ]
-    ends = [
-        pltpu.make_async_copy(src, dst, end_sems.at[n])
-        for n, (src, dst) in enumerate((
-            (taps_grad, taps_grad_hbm), (gain_grad, gain_grad_hbm), (bias_grad, bias_grad_hbm),
-            (weight, weight_grad_hbm),
-        ))
-    ]
-    for copy in extra[:2]:
+    for copy in loads:
         copy.start()
-    for n in range(seqs * seq_blocks):
-        s, here = n // seq_blocks, pl.ds(n % seq_blocks * rows, rows)
-        pairs = ((spread_hbm, spread), (values_hbm, values), (gates_hbm, gates))
-        loads.append([
-            pltpu.make_async_copy(src.at[s, here], dst.at[s, here], load_sems.at[m, n])
-            for m, (src, dst) in enumerate(pairs)
-        ])
-        for copy in loads[n]:
-            copy.start()
-    extra[2].start()
-    for copy in extra[:2]:
+    stores = []
+
+    def store(here, dst):
+        stores.append(pltpu.make_async_copy(here, dst, out_sems.at[len(stores)]))
+        stores[-1].start()
+
+    for copy, (_, here, dst) in zip(loads[1:], pairs[1:]):
         copy.wait()
+        store(here, dst)
+    loads[0].wait()
     taps_grad[...] = small[:K]
     bias_grad[...] = small[32:33]
     gain_grad[...] = small[33:34]
-    for copy in ends[:3]:
-        copy.start()
-    for n in range(seqs * seq_blocks):
-        s, first = n // seq_blocks, n % seq_blocks * rows
-        for copy in loads[n]:
-            copy.wait()
-        if n % seq_blocks == seq_blocks - 1:
-            spread[s, tokens - HALO :, :] += heads[s]
-        for i in range(rows // LANES):
-            here = slice(first + i * LANES, first + (i + 1) * LANES)
-            sig = sigmoid(gates[s, here, :].astype(F32))
-            values_part = spread[s, here, :] * sig
-            gates_part = values_part * values[s, here, :].astype(F32) * (1.0 - sig)
-            values[s, here, :] = values_part.astype(BF16)
-            gates[s, here, :] = gates_part.astype(BF16)
-        for m, (src, dst) in enumerate(((values, values_grad_hbm), (gates, gates_grad_hbm))):
-            copy = pltpu.make_async_copy(
-                src.at[s, pl.ds(first, rows)], dst.at[s, pl.ds(first, rows)], out_sems.at[m, n]
-            )
-            copy.start()
-            stores.append(copy)
-    extra[2].wait()
-    ends[3].start()
-    for copy in stores + ends:
+    store(taps_grad, taps_grad_hbm)
+    store(gain_grad, gain_grad_hbm)
+    store(bias_grad, bias_grad_hbm)
+    for copy in stores:
         copy.wait()
 
 
@@ -621,16 +626,17 @@
     def dma(*shape):
         return pltpu.SemaphoreType.DMA(shape)
 
+    one = pltpu.SemaphoreType.DMA
     anywhere = pl.BlockSpec(memory_space=pl.ANY)
     padded = windows * STEP + HALO
     block_sums = (2, rows // LANES, LANES)
-    spread, heads, small, weight_sum = pl.pallas_call(
+    values_sum, gates_sum, small, weight_sum = pl.pallas_call(
         functools.partial(fused_kernel, total_chans),
         in_specs=[anywhere] * 8,
         out_specs=[anywhere] * 4,
         out_shape=[
-            jax.ShapeDtypeStruct((seqs, tokens, chans), F32),
-            jax.ShapeDtypeStruct((seqs, HALO, chans), F32),
+            jax.ShapeDtypeStruct((seqs, tokens, chans), BF16),
+            jax.ShapeDtypeStruct((seqs, tokens, chans), BF16),
             jax.ShapeDtypeStruct((small_rows, chans), F32),
             jax.ShapeDtypeStruct((weight_rows, width), F32),
         ],
@@ -640,14 +646,14 @@
             pltpu.VMEM((seqs, HALO, chans), BF16),
             pltpu.VMEM((seqs, HALO, chans), BF16),
             pltpu.VMEM((positions, width), BF16),
-            pltpu.VMEM((chans, positions), BF16),
-            pltpu.VMEM((chans, width), BF16),
+            pltpu.VMEM((chans, max(positions, width)), BF16),
             pltpu.VMEM((width, chans), BF16),
             pltpu.VMEM((PAIR, groups, weight_rows, width), BF16),
             pltpu.VMEM((groups, weight_rows, width), BF16),
             pltpu.VMEM((groups - 1, weight_rows, width), BF16),
             pltpu.VMEM((groups - 1, weight_rows, width), BF16),
             pltpu.VMEM((weight_rows, width), F32),
+            pltpu.VMEM((seqs, tokens, chans), F32),
             pltpu.VMEM((seqs, tokens, chans), F32),
             pltpu.VMEM((2, rows, chans), F32),
             pltpu.VMEM((seqs, SPAN, chans), BF16),
@@ -666,8 +672,8 @@
             pltpu.VMEM((SPAN // 2, chans), F32),
             pltpu.VMEM((SPAN // 2, chans), F32),
             pltpu.VMEM((SPAN // 2, chans), F32),
-            pltpu.VMEM((seqs, HALO, chans), F32),
-            pltpu.VMEM((seqs, HALO, chans), F32),
+            pltpu.VMEM((seqs, HALO, chans), BF16),
+            pltpu.VMEM((seqs, HALO, chans), BF16),
             pltpu.VMEM((seqs, 2, chunks, LANES), F32),
             pltpu.VMEM((tp_others, seqs, 2, chunks, LANES), F32),
             pltpu.VMEM((seqs, chunks, LANES), F32),
@@ -677,26 +683,25 @@
             pltpu.VMEM((8, chans), F32),
             pltpu.VMEM((small_rows, chans), F32),
             pltpu.VMEM((small_rows, chans), F32),
+            pltpu.VMEM((small_rows, chans), F32),
             pltpu.VMEM((groups, small_rows, chans), F32),
             dma(2, seqs),
             dma(strips),
             dma(5),
-            dma(seqs),
-            dma(strips),
             dma(2),
             dma(2),
-            dma(tp_others, seqs),
-            dma(tp_others, seqs),
-            dma(tp_others, blocks),
-            dma(tp_others, blocks),
+            one,
+            dma(seqs),
+            one,
+            dma(seqs),
+            one,
             dma(parts),
-            dma(parts),
-            dma(groups - 1, parts),
-            dma(groups - 1, parts),
-            dma(seqs),
-            dma(seqs),
-            dma(groups),
-            dma(groups),
+            one,
+            one,
+            one,
+            one,
+            one,
+            dma(2),
         ],
         compiler_params=pltpu.CompilerParams(
             vmem_limit_bytes=VMEM_LIMIT, collective_id=0, has_side_effects=True
@@ -708,8 +713,8 @@
     )
 
     values_grad, gates_grad, weight_grad, taps_grad, gain_grad, bias_grad = pl.pallas_call(
-        finish_kernel,
-        in_specs=[anywhere] * 6,
+        hand_over_kernel,
+        in_specs=[anywhere] * 4,
         out_specs=[anywhere] * 6,
         out_shape=[
             jax.ShapeDtypeStruct((seqs, tokens, chans), BF16),
@@ -720,23 +725,19 @@
             jax.ShapeDtypeStruct((1, chans), F32),
         ],
         scratch_shapes=[
-            pltpu.VMEM((seqs, tokens, chans), F32),
             pltpu.VMEM((seqs, tokens, chans), BF16),
             pltpu.VMEM((seqs, tokens, chans), BF16),
             pltpu.VMEM((weight_rows, width), F32),
-            pltpu.VMEM((seqs, HALO, chans), F32),
             pltpu.VMEM((small_rows, chans), F32),
             pltpu.VMEM((K, chans), F32),
             pltpu.VMEM((1, chans), F32),
             pltpu.VMEM((1, chans), F32),
-            dma(3, blocks),
-            dma(2, blocks),
-            dma(3),
-            dma(4),
+            dma(2 * seqs + 2),
+            dma(2 * seqs + 4),
         ],
         compiler_params=pltpu.CompilerParams(vmem_limit_bytes=VMEM_LIMIT),
-        name="finish",
-    )(spread, values_in, gates_in, weight_sum, heads, small)
+        name="hand_over",
+    )(values_sum, gates_sum, weight_sum, small)
     return values_grad, gates_grad, taps_grad, gain_grad[0], bias_grad[0], weight_grad
 
 

time: 67 us -> 60.4 us (0.901)
  Pallas kernels: 66.2 us -> 59.6 us
    pallas_call x1, Pallas kernels: 60.1 us -> 55.4 us  [on_device(): pl.pallas_call(functools.partial(fused_kernel, total_chans), in_specs=[an...]
    pallas_call x1, Pallas kernels: 6.13 us -> 4.2 us  [on_device(): pl.pallas_call(hand_over_kernel, in_specs=[anywhere] * 4, out_specs=[anyw...]
where the time goes in v3:
time: 60.4 us; the launch traced here: 60.3 us
  Pallas kernels  59.6 us (99%)
  between operations  0.64 us (1%)
    pallas_call x1, Pallas kernels, on_device(): pl.pallas_call(functools.partial(fused_kernel, total_chans), in_specs=[an...  55.4 us
    pallas_call x1, Pallas kernels, on_device(): pl.pallas_call(hand_over_kernel, in_specs=[anywhere] * 4, out_specs=[anyw...  4.2 us

profile of v3, /device:TPU:0, one launch (start us, length us, event | category | flops | bytes accessed | tf_op | source)
XLA Modules:
  0.0 60.3 jit_solution(3408896788063793973)
XLA Ops:
  0.6 55.4 %fused.1 = (bf16[4,1024,256]{2,1,0:T(8,128)(2,1)}, bf16[4,1024,256]{2,1,0:T(8,128)(2,1)}, f32[40,256]{1,0:T(8,128)}, f32[32,4096]{1,0:T(8,128)}) custom-call(bf16[4,1024,256]{2,1,0:T(8,128)(2,1)} %values_hbm.1, bf16[4,1024,256]{2,1,0:T(8,128)(2,1)} %gates_hbm.1, bf16[4096,4096]{1,0:T(8,128)(2,1)} %bitcast.3, bf16[256,4096]{1,0:T(8,128)(2,1)} %weight_hbm.1, ...), custom_call_target="tpu_custom_call" | custom-call | tf_op jit(solution)/shard_map/fused/pallas_call | solution.py:633
  56.1 4.2 %hand_over.1 = (bf16[4,1024,256]{2,1,0:T(8,128)(2,1)}, bf16[4,1024,256]{2,1,0:T(8,128)(2,1)}, f32[32,4096]{1,0:T(8,128)}, f32[31,256]{1,0:T(8,128)}, f32[1,256]{1,0:T(1,128)}, /*index=5*/f32[1,256]{1,0:T(1,128)}) custom-call(bf16[4,1024,256]{2,1,0:T(8,128)(2,1)} %get-tuple-element.16.values_hbm, bf16[4,1024,256]{2,1,0:T(8,128)(2,1)} %get-tuple-element.17.gates_hbm, ...), custom_call_target="tpu_custom_call" | custom-call | tf_op jit(solution)/shard_map/hand_over/pallas_call | solution.py:715

commit v4 on v3

--- a/solution.py
+++ b/solution.py
@@ -12,6 +12,7 @@
 EPS = 1e-05
 HALO = 32
 PAIR = 2
+LAG = 4
 LANES = 128
 SPAN = 256
 STEP = SPAN - HALO
@@ -97,7 +98,7 @@
     onward, arrived, weight_sum, conv, norm_grad, grad, x_first, x_last, spectrum, high, low, grad_high, grad_low, table,
     taps, bias_row, gain_row, tap_rows,
     tap_re, tap_im, corr_re, corr_im, heads, heads_in, sums, sums_in, stat, back, back_in,
-    gain_acc, bias_acc, small, small_sum, small_total, small_in,
+    gain_acc, bias_acc, small, small_sum, small_in,
     load_sems, cot_sems, misc_sems, halo_send, halo_recv, sums_send, sums_recv,
     back_send, back_recv, pair_send, pair_recv, onward_send, onward_recv, head_send, head_recv,
     small_send, small_recv,
@@ -158,12 +159,17 @@
 
     greet([("tp", d) for d in tp_peers] + [("sp", d) for d in sp_peers])
     last = pl.ds(tokens - HALO, HALO)
-    halo_copies = [
-        remote(src.at[:, last], dst, halo_send.at[n], halo_recv.at[n], "sp", 1)
-        for n, (src, dst) in enumerate(((values_hbm, values_halo), (gates_hbm, gates_halo)))
-    ]
-    for copy in halo_copies:
-        copy.start()
+    halo_pairs = ((values_hbm, values_halo), (gates_hbm, gates_halo))
+
+    def halo_copies(s):
+        return [
+            remote(src.at[s, last], dst.at[s], halo_send.at[n], halo_recv.at[n, s], "sp", 1)
+            for n, (src, dst) in enumerate(halo_pairs)
+        ]
+
+    for s in range(seqs):
+        for copy in halo_copies(s):
+            copy.start()
 
     tail = tokens - (windows - 1) * STEP + HALO
     x_last[tail:, :] = jnp.zeros((SPAN - tail, chans), BF16)
@@ -227,13 +233,12 @@
 
     weight_load.wait()
     lax.fori_loop(0, width // 512, turn, 0)
-    for copy in halo_copies:
-        copy.wait()
     keep = jnp.where(me > 0, 1.0, 0.0).astype(F32)
-    for s in range(seqs):
+
+    def ahead(s, carry):
+        for copy in halo_copies(s):
+            copy.wait_recv()
         x_first[s, :HALO, :] = gate(values_halo[s].astype(F32) * keep, gates_halo[s])
-
-    def ahead(s, carry):
         x_last[:tail, :] = values[s, tokens - tail :, :]
         for w in range(windows):
             if w == 0:
@@ -347,7 +352,7 @@
 
         return carry
 
-    lag = min(3, strips)
+    lag = min(LAG, strips)
     strip_parts = parts // strips
     lax.fori_loop(0, strips, project, 0)
     passed = strips - lag
@@ -399,6 +404,9 @@
             copy.start()
 
     multiply(0)
+    if passed < parts:
+        pass_on(passed)
+        passed += 1
 
     def both(j, carry):
         middle(j - 1, j)
@@ -496,7 +504,7 @@
     small[33:34, :] = jnp.sum(gain_acc[...], axis=0, keepdims=True)
     small[34:, :] = jnp.zeros((small.shape[0] - 34, chans), F32)
     small_pair = remote(
-        small, small_in.at[0], pair_send, small_recv.at[0], "sp",
+        small, small_in, pair_send, small_recv.at[0], "sp",
         sp_devices + 1 - 2 * inner,
     )
     small_pair.start()
@@ -510,11 +518,13 @@
 
     lax.fori_loop(0, seqs, spread_rest, 0)
     small_pair.wait_recv()
-    small_sum[...] = small[...] + small_in[0]
-    small_copies = [
-        remote(small_sum, small_in.at[d], small_send, small_recv.at[1], "sp", d * PAIR)
-        for d in range(1, groups)
-    ]
+    small_sum[...] = (small[...] + small_in[...]).astype(BF16)
+    small_copies = []
+    for n in range(1, groups):
+        d = jnp.where(outer < groups // 2, groups - n, n)
+        small_copies.append(
+            remote(small_sum, small_hbm.at[d], small_send, small_recv.at[1], "sp", d * PAIR)
+        )
     for copy in small_copies:
         copy.start()
     keep_head = jnp.where(me < sp_devices - 1, 1.0, 0.0).astype(F32)
@@ -550,17 +560,13 @@
             pltpu.make_async_copy(
                 weight_sum.at[:, columns], weight_out_hbm.at[:, columns], misc_sems.at[2]
             ).start()
-    arrive(small_in.at[1:], small_recv.at[1], "sp")
-    total = small_sum[...]
-    for d in range(1, groups):
-        total = total + small_in[d]
-    small_total[...] = total
-    outs = [pltpu.make_async_copy(small_total, small_hbm, misc_sems.at[1])]
+    outs = [pltpu.make_async_copy(small_sum, small_hbm.at[0], misc_sems.at[1])]
     outs[0].start()
     for ref, sem, axis in (
+        (values_halo, halo_send.at[0], "sp"), (gates_halo, halo_send.at[1], "sp"),
         (sums_in, sums_send, "tp"), (back_in, back_send, "tp"), (onward, onward_send, "sp"),
         (pair, pair_send, "sp"), (small, pair_send, "sp"), (heads, head_send, "sp"),
-        (small_in.at[1:], small_send, "sp"),
+        (small_hbm.at[1:], small_send, "sp"),
     ):
         remote(ref, ref, sem, sem, axis, 1).wait_send()
     outs.append(pltpu.make_async_copy(weight_sum, weight_out_hbm, misc_sems.at[2]))
@@ -568,6 +574,7 @@
     outs.append(pltpu.make_async_copy(gates, gates_grad_hbm, misc_sems.at[4]))
     for copy in outs:
         copy.wait()
+    arrive(small_hbm.at[1:], small_recv.at[1], "sp")
 
 
 def hand_over_kernel(
@@ -596,9 +603,12 @@
         copy.wait()
         store(here, dst)
     loads[0].wait()
-    taps_grad[...] = small[:K]
-    bias_grad[...] = small[32:33]
-    gain_grad[...] = small[33:34]
+    total = small[0].astype(F32)
+    for d in range(1, small.shape[0]):
+        total = total + small[d].astype(F32)
+    taps_grad[...] = total[:K]
+    bias_grad[...] = total[32:33]
+    gain_grad[...] = total[33:34]
     store(taps_grad, taps_grad_hbm)
     store(gain_grad, gain_grad_hbm)
     store(bias_grad, bias_grad_hbm)
@@ -621,7 +631,7 @@
     sp_devices = lax.axis_size("sp")
     groups = sp_devices // PAIR
     weight_rows = chans // sp_devices
-    small_rows = 40
+    small_rows = 48
 
     def dma(*shape):
         return pltpu.SemaphoreType.DMA(shape)
@@ -637,7 +647,7 @@
         out_shape=[
             jax.ShapeDtypeStruct((seqs, tokens, chans), BF16),
             jax.ShapeDtypeStruct((seqs, tokens, chans), BF16),
-            jax.ShapeDtypeStruct((small_rows, chans), F32),
+            jax.ShapeDtypeStruct((groups, small_rows, chans), BF16),
             jax.ShapeDtypeStruct((weight_rows, width), F32),
         ],
         scratch_shapes=[
@@ -682,14 +692,13 @@
             pltpu.VMEM((8, chans), F32),
             pltpu.VMEM((8, chans), F32),
             pltpu.VMEM((small_rows, chans), F32),
+            pltpu.VMEM((small_rows, chans), BF16),
             pltpu.VMEM((small_rows, chans), F32),
-            pltpu.VMEM((small_rows, chans), F32),
-            pltpu.VMEM((groups, small_rows, chans), F32),
             dma(2, seqs),
             dma(strips),
             dma(5),
             dma(2),
-            dma(2),
+            dma(2, seqs),
             one,
             dma(seqs),
             one,
@@ -728,7 +737,7 @@
             pltpu.VMEM((seqs, tokens, chans), BF16),
             pltpu.VMEM((seqs, tokens, chans), BF16),
             pltpu.VMEM((weight_rows, width), F32),
-            pltpu.VMEM((small_rows, chans), F32),
+            pltpu.VMEM((groups, small_rows, chans), BF16),
             pltpu.VMEM((K, chans), F32),
             pltpu.VMEM((1, chans), F32),
             pltpu.VMEM((1, chans), F32),

time: 60.4 us -> 58.4 us (0.967)
  Pallas kernels: 59.6 us -> 57.6 us
    pallas_call x1, Pallas kernels: 55.4 us -> 53.4 us  [on_device(): pl.pallas_call(functools.partial(fused_kernel, total_chans), in_specs=[an...]
where the time goes in v4:
time: 58.4 us; the launch traced here: 58.2 us
  Pallas kernels  57.6 us (99%)
  between operations  0.64 us (1%)
    pallas_call x1, Pallas kernels, on_device(): pl.pallas_call(functools.partial(fused_kernel, total_chans), in_specs=[an...  53.4 us
    pallas_call x1, Pallas kernels, on_device(): pl.pallas_call(hand_over_kernel, in_specs=[anywhere] * 4, out_specs=[anyw...  4.23 us

profile of v4, /device:TPU:0, one launch (start us, length us, event | category | flops | bytes accessed | tf_op | source)
XLA Modules:
  0.0 58.2 jit_solution(17504415927900054920)
XLA Ops:
  0.6 53.4 %fused.1 = (bf16[4,1024,256]{2,1,0:T(8,128)(2,1)}, bf16[4,1024,256]{2,1,0:T(8,128)(2,1)}, bf16[4,48,256]{2,1,0:T(8,128)(2,1)}, f32[32,4096]{1,0:T(8,128)}) custom-call(bf16[4,1024,256]{2,1,0:T(8,128)(2,1)} %values_hbm.1, bf16[4,1024,256]{2,1,0:T(8,128)(2,1)} %gates_hbm.1, bf16[4096,4096]{1,0:T(8,128)(2,1)} %bitcast.3, bf16[256,4096]{1,0:T(8,128)(2,1)} %weight_hbm.1, ...), custom_call_target="tpu_custom_call" | custom-call | tf_op jit(solution)/shard_map/fused/pallas_call | solution.py:643
  54.0 4.2 %hand_over.1 = (bf16[4,1024,256]{2,1,0:T(8,128)(2,1)}, bf16[4,1024,256]{2,1,0:T(8,128)(2,1)}, f32[32,4096]{1,0:T(8,128)}, f32[31,256]{1,0:T(8,128)}, f32[1,256]{1,0:T(1,128)}, /*index=5*/f32[1,256]{1,0:T(1,128)}) custom-call(bf16[4,1024,256]{2,1,0:T(8,128)(2,1)} %get-tuple-element.16.values_hbm, bf16[4,1024,256]{2,1,0:T(8,128)(2,1)} %get-tuple-element.17.gates_hbm, ...), custom_call_target="tpu_custom_call" | custom-call | tf_op jit(solution)/shard_map/hand_over/pallas_call | solution.py:724
